TPU v7x, 32 devices: a whole 2x2x4 slice. The times are simulated.
32 devices in a mesh: sp: 4 (over z), fs: 4 (over y, x), tp: 2 (over core).
Axes of the slice: x: 2, y: 2, z: 4, core: 2. Of those that a mesh axis runs over, the one named last changes fastest.
Arguments:
- tokens: bfloat16 [4, 1024, 2048], P('fs', 'sp'), may hold values from -6 to 6
- norm_gain: float32 [2048], replicated, may hold values from 0.1 to 1.9
- query_weight: bfloat16 [2048, 1024], P(('sp', 'fs'), 'tp'), may hold values from -0.125 to 0.125
- key_weight: bfloat16 [2048, 1024], P(('sp', 'fs'), 'tp'), may hold values from -0.125 to 0.125
- value_weight: bfloat16 [2048, 1024], P(('sp', 'fs'), 'tp'), may hold values from -0.125 to 0.125
- outgate_weight: bfloat16 [2048, 1024], P(('sp', 'fs'), 'tp'), may hold values from -0.125 to 0.125
- gate_weight: bfloat16 [4, 8, 2048], P(None, 'tp'), may hold values from -0.125 to 0.125
- gate_bias: float32 [4, 8], P(None, 'tp'), may hold values from -1 to 100
- decay_extra: float32 [4, 2, 8, 1024], P('fs', None, 'tp', 'sp'), may hold values from -0.75 to 0
- init_memory: float32 [4, 2, 8, 128, 128], P('fs', None, 'tp'), may hold values from -48 to 48
- init_normalizer: float32 [4, 2, 8, 128], P('fs', None, 'tp'), may hold values from -48 to 48
- head_gain: float32 [8, 128], P('tp'), may hold values from 0.1 to 1.9
- pool_weight: bfloat16 [2048, 2048], P(('sp', 'fs'), 'tp'), may hold values from -0.125 to 0.125
- mem_out_weight: bfloat16 [2048, 1024], P(('sp', 'fs'), 'tp'), may hold values from -0.1875 to 0.1875
- pool_out_weight: bfloat16 [2048, 2048], P(('sp', 'fs'), 'tp'), may hold values from -0.125 to 0.125
Outputs:
- mixed: bfloat16 [4, 1024, 2048], P('fs', ('sp', 'tp'))
All inputs are finite; a program needn't handle non-finite values.
Results may differ from a plain program's by a relative error of at most 0.014.
Values may be sent and summed in bfloat16 or wider, within the bound.
A program may use at most 64 MiB of HBM per device.

v0:
```python
import functools
import math

import jax
import jax.numpy as jnp
from jax import lax
from jax.experimental import pallas as pl
from jax.experimental.pallas import tpu as pltpu
from jax.sharding import PartitionSpec as P

MESH = pl.DeviceIdType.MESH

HALO = 8


norm_eps = 1e-06
exact_mode = lax.Precision.HIGHEST


def carried_in(x, axis, combine, identity, reverse):
    length, position = (lax.axis_size(axis), lax.axis_index(axis))
    everything = jax.tree.map(lambda part: lax.all_gather(part, axis), x)
    start = jax.tree.map(
        lambda part, zero: jnp.broadcast_to(jnp.asarray(zero, part.dtype), part.shape), x, identity
    )

    def lap(k, before):
        at = length - 1 - k if reverse else k
        reached = at > position if reverse else at < position
        new = combine(before, jax.tree.map(lambda part: part[at], everything))
        return jax.tree.map(lambda a, b: jnp.where(reached, a, b), new, before)

    return lax.fori_loop(0, length, lap, start)


def padded_2(block, sides, width):
    for axis, dim in sides:
        count = lax.axis_size(axis)
        forward = [(i, i + 1) for i in range(count - 1)]
        backward = [(target, source) for source, target in forward]
        low = lax.ppermute(
            lax.slice_in_dim(block, block.shape[dim] - width, None, axis=dim), axis, forward
        )
        high = lax.ppermute(lax.slice_in_dim(block, 0, width, axis=dim), axis, backward)
        block = jnp.concatenate([low, block, high], axis=dim)
    return block


def block_output(
    query_rows, key_rows, value_rows, input_gate, log_forget, memory, normalizer, stabilizer
):
    block_len = query_rows.shape[1]
    key_scale = key_rows.shape[-1] ** (-0.5)
    lower_mask = jnp.tril(jnp.ones((block_len, block_len), dtype=bool))
    summed = jnp.cumsum(log_forget, axis=-1)
    log_decay = jnp.where(
        lower_mask, summed[:, :, None] - summed[:, None, :] + input_gate[:, None, :], -jnp.inf
    )
    log_carry = stabilizer[:, None] + summed
    running_max = jnp.maximum(log_carry, jnp.max(log_decay, axis=-1))
    scores = (
        jnp.einsum("btd,bsd->bts", query_rows, key_rows, preferred_element_type=jnp.float32)
        * key_scale
    )
    inner_weight = jnp.exp(log_decay - running_max[:, :, None]) * scores
    weight_rounded = inner_weight.astype(jnp.bfloat16)
    carry_weight = jnp.exp(log_carry - running_max)
    query_wide = query_rows.astype(jnp.float32)
    numerator = carry_weight[:, :, None] * jnp.einsum(
        "bed,btd->bte", memory, query_wide, precision=exact_mode
    )
    numerator = numerator + jnp.einsum(
        "bts,bse->bte", weight_rounded, value_rows, preferred_element_type=jnp.float32
    )
    denominator = carry_weight * jnp.einsum(
        "bd,btd->bt", normalizer, query_wide, precision=exact_mode
    )
    denominator = denominator + jnp.sum(inner_weight, axis=-1)
    return numerator / jnp.maximum(jnp.abs(denominator), jnp.exp(-running_max))[:, :, None]


def block_summary(key_rows, value_rows, input_gate, log_forget):
    key_wide = key_rows.astype(jnp.float32) * key_rows.shape[-1] ** (-0.5)
    summed = jnp.cumsum(log_forget, axis=-1)
    forget_total = summed[:, -1]
    log_weight = forget_total[:, None] - summed + input_gate
    running_max = jnp.max(log_weight, axis=-1)
    weights = jnp.exp(log_weight - running_max[:, None])
    memory = jnp.einsum(
        "bse,bsd->bed",
        weights[:, :, None] * value_rows.astype(jnp.float32),
        key_wide,
        precision=exact_mode,
    )
    normalizer = jnp.einsum("bs,bsd->bd", weights, key_wide, precision=exact_mode)
    return (memory, normalizer, running_max, forget_total)


def combine(earlier, latter):
    early_memory, early_norm, early_max, early_total = earlier
    late_memory, late_norm, late_max, late_total = latter
    joint_max = jnp.maximum(early_max + late_total, late_max)
    early_scale = jnp.exp(early_max + late_total - joint_max)
    late_scale = jnp.exp(late_max - joint_max)
    memory = early_scale[:, None, None] * early_memory + late_scale[:, None, None] * late_memory
    normalizer = early_scale[:, None] * early_norm + late_scale[:, None] * late_norm
    return (memory, normalizer, joint_max, early_total + late_total)


def span_sweep(
    query_rows, key_rows, value_rows, input_gate, log_forget, memory, normalizer, stabilizer, span
):
    block_count = query_rows.shape[1] // span

    def to_blocks(array):
        shaped = array.reshape((array.shape[0], block_count, span) + array.shape[2:])
        return jnp.moveaxis(shaped, 1, 0)

    def advance(carried, pieces):
        query_blk, key_blk, value_blk, gate_blk, forget_blk = pieces
        result = block_output(
            query_blk, key_blk, value_blk, gate_blk, forget_blk, carried[0], carried[1], carried[2]
        )
        return (combine(carried, block_summary(key_blk, value_blk, gate_blk, forget_blk)), result)

    initial = (memory, normalizer, stabilizer, jnp.zeros_like(stabilizer))
    ignored, outputs = lax.scan(
        advance,
        initial,
        tuple(
            (
                to_blocks(array)
                for array in (query_rows, key_rows, value_rows, input_gate, log_forget)
            )
        ),
    )
    return jnp.moveaxis(outputs, 0, 1).reshape(query_rows.shape[:2] + (value_rows.shape[2],))


def reverse_time(array):
    return jnp.flip(array, axis=1)


def to_heads(matrix, head_count):
    shaped = matrix.reshape(matrix.shape[0], head_count, matrix.shape[1] // head_count)
    return shaped.transpose(1, 0, 2)


def pool_window(padded, positions, channels, seq_len, group_size):
    row_count = positions.shape[0]
    group_index = channels // group_size
    reach_left = jnp.left_shift(jnp.ones_like(group_index), group_index)
    reach_right = reach_left - 1
    window_sum = jnp.zeros((row_count, channels.shape[0]), jnp.float32)
    for offset in range(-HALO, HALO):
        inside = ((offset >= -reach_left) & (offset <= reach_right)).astype(jnp.float32)
        window_sum = window_sum + inside * padded[HALO + offset : HALO + offset + row_count]
    first_pos = jnp.maximum(positions[:, None] - reach_left[None, :], 0)
    last_pos = jnp.minimum(positions[:, None] + reach_right[None, :], seq_len - 1)
    counted = (last_pos - first_pos + 1).astype(jnp.float32)
    centre = padded[HALO : HALO + row_count]
    return (window_sum / counted - centre).astype(jnp.bfloat16)


def per_device(
    tokens,
    norm_gain,
    query_weight,
    key_weight,
    value_weight,
    outgate_weight,
    gate_weight,
    gate_bias,
    decay_extra,
    init_memory,
    init_normalizer,
    head_gain,
    pool_weight,
    mem_out_weight,
    pool_out_weight,
):
    block_len = tokens.shape[1]
    model_width = tokens.shape[2]
    head_count, head_width = head_gain.shape
    span = math.gcd(block_len, 256)
    flattened = tokens[0].astype(jnp.float32)
    normed = (
        flattened
        * lax.rsqrt(jnp.mean(flattened * flattened, axis=-1, keepdims=True) + norm_eps)
        * norm_gain
    ).astype(jnp.bfloat16)
    zero_start = tuple(
        (
            jnp.zeros((block_len, weight.shape[1]), jnp.float32)
            for weight in (query_weight, key_weight, value_weight, outgate_weight, pool_weight)
        )
    )
    zero_start = zero_start + (
        jnp.zeros((model_width, mem_out_weight.shape[1]), jnp.bfloat16),
        jnp.zeros((model_width, pool_out_weight.shape[1]), jnp.bfloat16),
    )
    line_query, line_key, line_value, line_outgate, line_pool, line_mem_out, line_pool_out = (
        lax.all_gather(query_weight, "fs", axis=0, tiled=True),
        lax.all_gather(key_weight, "fs", axis=0, tiled=True),
        lax.all_gather(value_weight, "fs", axis=0, tiled=True),
        lax.all_gather(outgate_weight, "fs", axis=0, tiled=True),
        lax.all_gather(pool_weight, "fs", axis=0, tiled=True),
        lax.all_gather(mem_out_weight, "fs", axis=0, tiled=True),
        lax.all_gather(pool_out_weight, "fs", axis=0, tiled=True),
    )
    pieces = (
        lax.all_gather(line_query, "sp", axis=0, tiled=True),
        lax.all_gather(line_key, "sp", axis=0, tiled=True),
        lax.all_gather(line_value, "sp", axis=0, tiled=True),
        lax.all_gather(line_outgate, "sp", axis=0, tiled=True),
        lax.all_gather(line_pool, "sp", axis=0, tiled=True),
        lax.all_gather(line_mem_out, "sp", axis=0, tiled=True),
        lax.all_gather(line_pool_out, "sp", axis=0, tiled=True),
    )
    partial_sums = tuple(
        (
            jnp.dot(normed, weight_rows, preferred_element_type=jnp.float32)
            for weight_rows in pieces[:5]
        )
    )
    collected = tuple((weight_rows for weight_rows in pieces[5:]))
    folded = partial_sums + collected
    query_proj, key_proj, value_proj, outgate, pool_input = tuple(
        (running.astype(jnp.bfloat16) for running in folded[:5])
    )
    mem_weight_all = folded[5]
    pool_weight_all = folded[6]
    gate_pre = lax.dot_general(
        normed,
        gate_weight.reshape(4 * head_count, model_width),
        (((1,), (1,)), ((), ())),
        preferred_element_type=jnp.float32,
    ) + gate_bias.reshape(4 * head_count)
    gate_pre = gate_pre.reshape(block_len, 4, head_count).transpose(1, 2, 0)
    query_heads = to_heads(query_proj, head_count)
    key_heads = to_heads(key_proj, head_count)
    value_heads = to_heads(value_proj, head_count)
    forward_forget = jax.nn.log_sigmoid(gate_pre[1]) + decay_extra[0, 0]
    backward_forget = jax.nn.log_sigmoid(gate_pre[3]) + decay_extra[0, 1]
    zero_rows = jnp.zeros((head_count,), jnp.float32)
    identity = (
        jnp.zeros((head_count, head_width, head_width), jnp.float32),
        jnp.zeros((head_count, head_width), jnp.float32),
        jnp.full((head_count,), -1e30, jnp.float32),
        zero_rows,
    )
    front_memory, front_norm, front_max, front_total = block_summary(
        key_heads, value_heads, gate_pre[0], forward_forget
    )
    prefix = carried_in(
        (front_memory, front_norm, front_max, front_total), "sp", combine, identity, False
    )
    incoming = combine((init_memory[0, 0], init_normalizer[0, 0], zero_rows, zero_rows), prefix)
    forward_out = span_sweep(
        query_heads,
        key_heads,
        value_heads,
        gate_pre[0],
        forward_forget,
        incoming[0],
        incoming[1],
        incoming[2],
        span,
    )
    back_query = reverse_time(query_heads)
    back_key = reverse_time(key_heads)
    back_value = reverse_time(value_heads)
    back_gate = reverse_time(gate_pre[2])
    back_forget = reverse_time(backward_forget)
    rear_memory, rear_norm, rear_max, rear_total = block_summary(
        back_key, back_value, back_gate, back_forget
    )
    suffix = carried_in(
        (rear_memory, rear_norm, rear_max, rear_total), "sp", combine, identity, True
    )
    back_incoming = combine(
        (init_memory[0, 1], init_normalizer[0, 1], zero_rows, zero_rows), suffix
    )
    backward_out = reverse_time(
        span_sweep(
            back_query,
            back_key,
            back_value,
            back_gate,
            back_forget,
            back_incoming[0],
            back_incoming[1],
            back_incoming[2],
            span,
        )
    )
    summed_dirs = (forward_out + backward_out).transpose(1, 0, 2)
    normed_heads = (
        summed_dirs
        * lax.rsqrt(jnp.mean(summed_dirs * summed_dirs, axis=-1, keepdims=True) + norm_eps)
        * head_gain
    )
    out_gate = jax.nn.sigmoid(
        outgate.astype(jnp.float32).reshape(block_len, head_count, head_width)
    )
    memory_out = (
        (normed_heads * out_gate).astype(jnp.bfloat16).reshape(block_len, head_count * head_width)
    )
    padded = padded_2(pool_input, (("sp", 0),), HALO).astype(jnp.float32)
    feature_count = pool_input.shape[1]
    positions = lax.axis_index("sp") * block_len + jnp.arange(block_len, dtype=jnp.int32)
    channels = lax.axis_index("tp") * feature_count + jnp.arange(feature_count, dtype=jnp.int32)
    pool_out = pool_window(
        padded, positions, channels, block_len * lax.axis_size("sp"), model_width // 4
    )
    own_rows = block_len // lax.axis_size("tp")
    result = lax.dot_general(
        memory_out, mem_weight_all, (((1,), (1,)), ((), ())), preferred_element_type=jnp.float32
    )
    mixed = lax.psum_scatter(
        (
            result
            + lax.dot_general(
                pool_out,
                pool_weight_all,
                (((1,), (1,)), ((), ())),
                preferred_element_type=jnp.float32,
            )
        ).astype(jnp.bfloat16),
        "tp",
        scatter_dimension=0,
        tiled=True,
    )
    return mixed.reshape(1, own_rows, model_width)


def aligned(start, size):
    return pl.ds(pl.multiple_of(start, size), size)


def gather_kernel(n_sp, n_fs, widths, *refs):
    count = len(widths)
    token_ref, decay_ref = refs[:2]
    weight_refs = refs[2 : 2 + count]
    x_ref, decay_out, in_ref, out_ref = refs[2 + count : 6 + count]
    (
        local_sem,
        token_local,
        weight_send,
        weight_recv,
        decay_send,
        decay_recv,
        token_send,
        token_recv,
        swap_send,
        swap_recv,
        row_send,
        row_recv,
        relay_send,
        relay_recv,
    ) = refs[6 + count :]
    sp, fs, tp = (lax.axis_index(name) for name in ("sp", "fs", "tp"))
    other = 1 - tp
    rows = weight_refs[0].shape[0]
    block = token_ref.shape[0]
    half = block // 2
    ups = [lax.rem(sp + k, n_sp) for k in range(n_sp)]
    downs = [lax.rem(sp + n_sp - k, n_sp) for k in range(n_sp)]
    beside = fs + 1 - 2 * lax.rem(fs, 2)
    across = lax.rem(fs + 2, 4)
    peers = (beside, across)

    barrier = pltpu.get_barrier_semaphore()
    for k in range(1, n_sp):
        pl.semaphore_signal(barrier, inc=1, device_id={"sp": ups[k]}, device_id_type=MESH)
    for peer in peers:
        pl.semaphore_signal(barrier, inc=1, device_id={"fs": peer}, device_id_type=MESH)
    pl.semaphore_signal(barrier, inc=1, device_id={"tp": other}, device_id_type=MESH)
    pl.semaphore_wait(barrier, n_sp + 2)

    in_count = count - 2
    in_width = sum(widths[:in_count])

    def landing(i, source_sp):
        at = aligned((source_sp * n_fs + fs) * rows, rows)
        start = sum(widths[:i])
        if i < in_count:
            return in_ref.at[at, pl.ds(start, widths[i])]
        return out_ref.at[at, pl.ds(start - in_width, widths[i])]

    def piece(i, target_sp):
        return weight_refs[i].at[:, aligned(target_sp * widths[i], widths[i])]

    locals_ = []
    for i in range(count):
        locals_.append(pltpu.make_async_copy(piece(i, sp), landing(i, sp), local_sem.at[i]))
    for copy in locals_:
        copy.start()
    own_tokens = pltpu.make_async_copy(
        token_ref, x_ref.at[aligned(sp * block, block)], token_local.at[0]
    )
    own_tokens.start()
    own_decay = pltpu.make_async_copy(decay_ref.at[sp], decay_out.at[sp], token_local.at[1])
    own_decay.start()

    def weight_copy(i, k, target, source):
        return pltpu.make_async_remote_copy(
            src_ref=piece(i, target),
            dst_ref=landing(i, source),
            send_sem=weight_send.at[k - 1, i],
            recv_sem=weight_recv.at[k - 1, i],
            device_id={"sp": target},
            device_id_type=MESH,
        )

    def decay_copy(k, target, source):
        return pltpu.make_async_remote_copy(
            src_ref=decay_ref.at[target],
            dst_ref=decay_out.at[source],
            send_sem=decay_send.at[k - 1],
            recv_sem=decay_recv.at[k - 1],
            device_id={"sp": target},
            device_id_type=MESH,
        )

    def token_copy(source, step):
        at = aligned(source * block + tp * half, half)
        return pltpu.make_async_remote_copy(
            src_ref=token_ref.at[aligned(tp * half, half)] if source is sp else x_ref.at[at],
            dst_ref=x_ref.at[at],
            send_sem=token_send.at[source * 2 + (step + 1) // 2],
            recv_sem=token_recv.at[source],
            device_id={"sp": sp + step},
            device_id_type=MESH,
        )

    def swap_copy(source, side):
        at = x_ref.at[aligned(source * block + side * half, half)]
        return pltpu.make_async_remote_copy(
            src_ref=at,
            dst_ref=at,
            send_sem=swap_send.at[source],
            recv_sem=swap_recv.at[source],
            device_id={"tp": other},
            device_id_type=MESH,
        )

    def row_copies(k, j, at_fs):
        at = aligned((downs[k] * n_fs + at_fs) * rows, rows)
        return [
            pltpu.make_async_remote_copy(
                src_ref=ref.at[at],
                dst_ref=ref.at[at],
                send_sem=row_send.at[k, j, which],
                recv_sem=row_recv.at[k, j, which],
                device_id={"fs": peers[j]},
                device_id_type=MESH,
            )
            for which, ref in enumerate((in_ref, out_ref))
        ]

    def relay_copies(k, j, at_fs):
        part = rows // 2
        at = aligned((downs[k] * n_fs + at_fs) * rows + j * part, part)
        return [
            pltpu.make_async_remote_copy(
                src_ref=ref.at[at],
                dst_ref=ref.at[at],
                send_sem=relay_send.at[k, j, which],
                recv_sem=relay_recv.at[k, j, which],
                device_id={"fs": peers[j]},
                device_id_type=MESH,
            )
            for which, ref in enumerate((in_ref, out_ref))
        ]

    def neighbour_sends(action):
        for step in (1, -1):
            @pl.when((sp + step >= 0) & (sp + step < n_sp))
            def _(step=step):
                action(token_copy(sp, step))

    def arrivals(action, distances):
        for distance in distances:
            for step in (1, -1):
                source = sp - step * distance
                onward = sp + step

                @pl.when((source >= 0) & (source < n_sp))
                def _(source=source, onward=onward, step=step):
                    action(source, onward, step)

    def relay_tokens(source, onward, step):
        token_copy(source, step).wait_recv()
        swap_copy(source, tp).start()

        @pl.when((onward >= 0) & (onward < n_sp))
        def _():
            token_copy(source, step).start()

    def finish_tokens(source, onward, step):
        swap_copy(source, other).wait_recv()
        swap_copy(source, tp).wait_send()

        @pl.when((onward >= 0) & (onward < n_sp))
        def _():
            token_copy(source, step).wait_send()

    for k in range(1, n_sp):
        for i in range(count):
            weight_copy(i, k, ups[k], sp).start()
    for k in range(1, n_sp):
        decay_copy(k, ups[k], sp).start()
    neighbour_sends(lambda copy: copy.start())
    for copy in locals_:
        copy.wait()
    for k in range(n_sp):
        if k:
            for i in range(count):
                weight_copy(i, k, ups[k], downs[k]).wait_recv()
        for j in range(2):
            for copy in row_copies(k, j, fs):
                copy.start()
    for k in range(n_sp):
        for j in range(2):
            for copy in row_copies(k, j, peers[j]):
                copy.wait_recv()
            for copy in relay_copies(k, 1 - j, peers[j]):
                copy.start()
        if k == n_sp - 2:
            arrivals(relay_tokens, (1,))
    arrivals(relay_tokens, range(2, n_sp))
    own_tokens.wait()
    own_decay.wait()
    for k in range(1, n_sp):
        decay_copy(k, ups[k], downs[k]).wait_recv()
    for k in range(n_sp):
        for j in range(2):
            for copy in relay_copies(k, j, 3 - fs):
                copy.wait_recv()
    arrivals(finish_tokens, range(1, n_sp))
    neighbour_sends(lambda copy: copy.wait_send())
    for k in range(1, n_sp):
        for i in range(count):
            weight_copy(i, k, ups[k], sp).wait_send()
        decay_copy(k, ups[k], sp).wait_send()
    for k in range(n_sp):
        for j in range(2):
            for copy in row_copies(k, j, fs):
                copy.wait_send()
            for copy in relay_copies(k, j, peers[1 - j]):
                copy.wait_send()


def gather_all(tokens, decay, weights):
    n_sp, n_fs = lax.axis_size("sp"), lax.axis_size("fs")
    widths = tuple(weight.shape[1] // n_sp for weight in weights)
    block, model_width = tokens.shape
    count = len(weights)
    vmem = pl.BlockSpec(memory_space=pltpu.VMEM)
    dma = pltpu.SemaphoreType.DMA
    return pl.pallas_call(
        functools.partial(gather_kernel, n_sp, n_fs, widths),
        out_shape=(
            jax.ShapeDtypeStruct((n_sp * block, model_width), tokens.dtype),
            jax.ShapeDtypeStruct(decay.shape, decay.dtype),
            jax.ShapeDtypeStruct((model_width, sum(widths[:-2])), tokens.dtype),
            jax.ShapeDtypeStruct((model_width, sum(widths[-2:])), tokens.dtype),
        ),
        in_specs=[pl.BlockSpec(memory_space=pl.ANY)] * (2 + count),
        out_specs=(vmem,) * 4,
        scratch_shapes=[
            dma((count,)),
            dma((2,)),
            dma((n_sp - 1, count)),
            dma((n_sp - 1, count)),
            dma((n_sp - 1,)),
            dma((n_sp - 1,)),
            dma((2 * n_sp,)),
            dma((n_sp,)),
            dma((n_sp,)),
            dma((n_sp,)),
            dma((n_sp, 2, 2)),
            dma((n_sp, 2, 2)),
            dma((n_sp, 2, 2)),
            dma((n_sp, 2, 2)),
        ],
        compiler_params=pltpu.CompilerParams(
            collective_id=0, has_side_effects=True, vmem_limit_bytes=60 * 2**20
        ),
        name="gather_all",
    )(tokens, decay, *weights)


def input_kernel(x_ref, gain_ref, weight_ref, gates_ref, bias_ref, proj_ref, pre_ref):
    wide = x_ref[...].astype(jnp.float32)
    normed = (
        wide
        * lax.rsqrt(jnp.mean(wide * wide, axis=-1, keepdims=True) + norm_eps)
        * gain_ref[...]
    ).astype(jnp.bfloat16)
    proj_ref[...] = jnp.dot(
        normed, weight_ref[...], preferred_element_type=jnp.float32
    ).astype(jnp.bfloat16)
    pre_ref[...] = (
        lax.dot_general(
            normed, gates_ref[...], (((1,), (1,)), ((), ())), preferred_element_type=jnp.float32
        )
        + bias_ref[...]
    )


def project_in(x, norm_gain, weight, gates, bias):
    seq, width = x.shape
    tb = math.gcd(seq, 256)

    def fixed(array):
        return pl.BlockSpec(array.shape, lambda t: (0, 0))

    def rows(columns):
        return pl.BlockSpec((tb, columns), lambda t: (t, 0))

    norm_gain = norm_gain[None]
    return pl.pallas_call(
        input_kernel,
        grid=(seq // tb,),
        out_shape=(
            jax.ShapeDtypeStruct((seq, weight.shape[1]), jnp.bfloat16),
            jax.ShapeDtypeStruct((seq, gates.shape[0]), jnp.float32),
        ),
        in_specs=[rows(width), fixed(norm_gain), fixed(weight), fixed(gates), fixed(bias)],
        out_specs=(rows(weight.shape[1]), rows(gates.shape[0])),
        name="project_in",
    )(x, norm_gain, weight, gates, bias)


def scan_lanes(x, combine_, fill, reverse):
    length = x.shape[1]
    lane = lax.broadcasted_iota(jnp.int32, x.shape, 1)
    d = 1
    while d < length:
        if reverse:
            moved = jnp.where(lane < length - d, pltpu.roll(x, length - d, 1), fill)
        else:
            moved = jnp.where(lane >= d, pltpu.roll(x, d, 1), fill)
        x = combine_(x, moved)
        d *= 2
    return x


def prepare_gates(pre_ref, decay_ref, cols_ref, rows_ref, flat_ref):
    gates = pre_ref[...].T[:8]
    forget = jnp.minimum(gates, 0.0) - jnp.log1p(jnp.exp(-jnp.abs(gates))) + decay_ref[...]
    front_sum = scan_lanes(forget, jnp.add, 0.0, False)[1:2]
    rear_sum = scan_lanes(forget, jnp.add, 0.0, True)[3:4]
    front_level = gates - front_sum
    rear_level = gates - rear_sum
    front_peak = scan_lanes(front_level, jnp.maximum, 0.0, False)[0:1]
    rear_peak = scan_lanes(rear_level, jnp.maximum, 0.0, True)[2:3]
    front_peak = jnp.maximum(front_peak, 0.0)
    rear_peak = jnp.maximum(rear_peak, 0.0)
    rows_ref[0:1, :] = front_level[0:1]
    rows_ref[1:2, :] = rear_level[2:3]
    flat_ref[...] = jnp.zeros_like(flat_ref)
    flat_ref[0:1, :] = front_peak
    flat_ref[1:2, :] = rear_peak
    flat_ref[2:3, :] = front_sum + front_peak
    flat_ref[3:4, :] = rear_sum + rear_peak
    flat_ref[4:5, :] = rear_level[2:3]
    cols_ref[...] = flat_ref[...].T


def memory_kernel(
    q_ref, qk_ref, k_ref, v_ref, gate_ref, pre_ref, decay_ref, mem_ref, norm_ref, gain_ref, o_ref,
    cols_ref, rows_ref, flat_ref,
):
    @pl.when(pl.program_id(0) == 0)
    def _():
        prepare_gates(pre_ref, decay_ref, cols_ref, rows_ref, flat_ref)

    tb = q_ref.shape[0]
    seq = k_ref.shape[0]
    width = q_ref.shape[1]
    scale = width ** (-0.5)
    q = q_ref[...]
    cols = cols_ref[pl.ds(pl.multiple_of(pl.program_id(0) * tb, tb), tb), :]
    front_peak, rear_peak = cols[:, 0:1], cols[:, 1:2]
    front_max, rear_max = cols[:, 2:3], cols[:, 3:4]
    rear_own = cols[:, 4:5]
    score = (
        lax.dot_general(
            q, k_ref[...], (((1,), (1,)), ((), ())), preferred_element_type=jnp.float32
        )
        * scale
    )
    t = pl.program_id(0) * tb + lax.broadcasted_iota(jnp.int32, (tb, seq), 0)
    s = lax.broadcasted_iota(jnp.int32, (tb, seq), 1)
    front = s <= t
    weight = (
        jnp.exp(
            jnp.where(front, rows_ref[0:1, :] - front_peak, rows_ref[1:2, :] - rear_peak)
        )
        * score
    )
    front_weight = jnp.where(front, weight, 0.0)
    rear_weight = jnp.where(front, 0.0, weight)
    wide = q.astype(jnp.float32)
    own_score = jnp.sum(wide * qk_ref[...].astype(jnp.float32), axis=1, keepdims=True) * scale
    own_weight = jnp.exp(rear_own - rear_peak) * own_score
    start = t.shape[0] * pl.program_id(0)
    own_value = v_ref[pl.ds(pl.multiple_of(start, tb), tb), :].astype(jnp.float32)
    carry = lax.dot_general(
        wide,
        mem_ref[...],
        (((1,), (1,)), ((), ())),
        precision=exact_mode,
        preferred_element_type=jnp.float32,
    )

    def one(direction, weights, peak, top, extra_num, extra_den):
        decay = jnp.exp(-peak)
        num = decay * carry[:, direction * width : (direction + 1) * width] + jnp.dot(
            weights.astype(jnp.bfloat16), v_ref[...], preferred_element_type=jnp.float32
        )
        den = decay * jnp.sum(
            wide * norm_ref[direction : direction + 1, :], axis=1, keepdims=True
        ) + jnp.sum(weights, axis=1, keepdims=True)
        return (num + extra_num) / jnp.maximum(jnp.abs(den + extra_den), jnp.exp(-top))

    total = one(0, front_weight, front_peak, front_max, 0.0, 0.0) + one(
        1,
        rear_weight,
        rear_peak,
        rear_max,
        own_weight.astype(jnp.bfloat16).astype(jnp.float32) * own_value,
        own_weight,
    )
    normed = (
        total
        * lax.rsqrt(jnp.mean(total * total, axis=-1, keepdims=True) + norm_eps)
        * gain_ref[...]
    )
    o_ref[...] = (normed * jax.nn.sigmoid(gate_ref[...].astype(jnp.float32))).astype(jnp.bfloat16)


def memory_mix(proj, pre, decay, memory, normalizer, gain, width):
    seq = proj.shape[0]
    tb = math.gcd(seq, 256)

    def part(i, whole):
        if whole:
            return pl.BlockSpec((seq, width), lambda t: (0, i))
        return pl.BlockSpec((tb, width), lambda t: (t, i))

    def fixed(array):
        return pl.BlockSpec(array.shape, lambda t: (0, 0))

    return pl.pallas_call(
        memory_kernel,
        grid=(seq // tb,),
        out_shape=jax.ShapeDtypeStruct((seq, width), jnp.bfloat16),
        in_specs=[
            part(0, False),
            part(1, False),
            part(1, True),
            part(2, True),
            part(3, False),
            fixed(pre),
            fixed(decay),
            fixed(memory),
            fixed(normalizer),
            fixed(gain),
        ],
        out_specs=pl.BlockSpec((tb, width), lambda t: (t, 0)),
        scratch_shapes=[
            pltpu.VMEM((seq, 128), jnp.float32),
            pltpu.VMEM((8, seq), jnp.float32),
            pltpu.VMEM((128, seq), jnp.float32),
        ],
        name="memory_mix",
    )(proj, proj, proj, proj, proj, pre, decay, memory, normalizer, gain)


def project_kernel(
    n_sp, mem_ref, pool_ref, weight_ref, o_ref,
    give, take, send, land, total, own, swap_send, swap_recv, z_send, z_recv,
):
    sp, tp = lax.axis_index("sp"), lax.axis_index("tp")
    other = 1 - tp
    half = o_ref.shape[0]
    width = o_ref.shape[1]
    split = mem_ref.shape[1]
    tile = math.gcd(width, 512)

    barrier = pltpu.get_barrier_semaphore()
    for k in range(1, n_sp):
        pl.semaphore_signal(
            barrier, inc=1, device_id={"sp": lax.rem(sp + k, n_sp)}, device_id_type=MESH
        )
    pl.semaphore_signal(barrier, inc=1, device_id={"tp": other}, device_id_type=MESH)
    pl.semaphore_wait(barrier, n_sp)

    def product(target, side, c):
        at = aligned(target * 2 * half + side * half, half)
        columns = pl.ds(c * tile, tile)
        dims = (((1,), (1,)), ((), ()))
        return lax.dot_general(
            mem_ref[at, :],
            weight_ref[columns, :split],
            dims,
            preferred_element_type=jnp.float32,
        ) + lax.dot_general(
            pool_ref[at, :],
            weight_ref[columns, split:],
            dims,
            preferred_element_type=jnp.float32,
        )

    def swap(d):
        return pltpu.make_async_remote_copy(
            src_ref=give.at[d],
            dst_ref=take.at[d],
            send_sem=swap_send.at[d],
            recv_sem=swap_recv.at[d],
            device_id={"tp": other},
            device_id_type=MESH,
        )

    low = 1 - (2 * sp) // n_sp
    place = low * sp + (1 - low) * (n_sp - 1 - sp)

    def pass_on(d, up):
        slot = up * n_sp + d
        return pltpu.make_async_remote_copy(
            src_ref=send.at[d],
            dst_ref=land.at[slot],
            send_sem=z_send.at[d],
            recv_sem=z_recv.at[slot],
            device_id={"sp": sp + 2 * up - 1},
            device_id_type=MESH,
        )

    def actual(d):
        return low * d + (1 - low) * (n_sp - 1 - d)

    order = [(d, actual(d)) for d in range(n_sp - 1, -1, -1)]
    tiles = [slice(c * tile, (c + 1) * tile) for c in range(width // tile)]
    for _, target in order:
        for c, at in enumerate(tiles):
            give[target, :, at] = product(target, other, c).astype(jnp.bfloat16)
        swap(target).start()
    for d, target in order:
        swap(target).wait_recv()
        for c, at in enumerate(tiles):
            total[:, at] = product(target, tp, c) + take[target, :, at].astype(jnp.float32)

        @pl.when(place == d)
        def _():
            own[...] = total[...]

        def forward(up, fed, target=target):
            @pl.when(fed)
            def _():
                pass_on(target, up).wait_recv()
                total[...] += land[up * n_sp + target].astype(jnp.float32)

            send[target] = total[...].astype(jnp.bfloat16)
            pass_on(target, up).start()

        @pl.when(place < d)
        def _():
            forward(low, place > 0)

        @pl.when(place > d)
        def _():
            forward(1 - low, place < n_sp - 1)

    for up in (0, 1):
        @pl.when(sp != (n_sp - 1) * (1 - up))
        def _(up=up):
            pass_on(sp, up).wait_recv()
            own[...] += land[up * n_sp + sp].astype(jnp.float32)

    o_ref[...] = own[...].astype(jnp.bfloat16)
    for d, target in order:
        swap(target).wait_send()

        @pl.when(place != d)
        def _(target=target):
            pass_on(target, 0).wait_send()


def project_out(memory_out, pool_out, weight):
    n_sp = lax.axis_size("sp")
    half = memory_out.shape[0] // (2 * n_sp)
    width = weight.shape[0]
    vmem = pl.BlockSpec(memory_space=pltpu.VMEM)
    dma = pltpu.SemaphoreType.DMA
    buffers = pltpu.VMEM((n_sp, half, width), jnp.bfloat16)
    return pl.pallas_call(
        functools.partial(project_kernel, n_sp),
        out_shape=jax.ShapeDtypeStruct((half, width), jnp.bfloat16),
        in_specs=[vmem] * 3,
        out_specs=vmem,
        scratch_shapes=[
            buffers,
            buffers,
            buffers,
            pltpu.VMEM((2 * n_sp, half, width), jnp.bfloat16),
            pltpu.VMEM((half, width), jnp.float32),
            pltpu.VMEM((half, width), jnp.float32),
            dma((n_sp,)),
            dma((n_sp,)),
            dma((n_sp,)),
            dma((2 * n_sp,)),
        ],
        compiler_params=pltpu.CompilerParams(
            collective_id=1, has_side_effects=True, vmem_limit_bytes=40 * 2**20
        ),
        name="project_out",
    )(memory_out, pool_out, weight)


def by_head(
    tokens,
    norm_gain,
    query_weight,
    key_weight,
    value_weight,
    outgate_weight,
    gate_weight,
    gate_bias,
    decay_extra,
    init_memory,
    init_normalizer,
    head_gain,
    pool_weight,
    mem_out_weight,
    pool_out_weight,
):
    model_width = tokens.shape[2]
    width = head_gain.shape[1]
    n_sp = lax.axis_size("sp")
    sp, tp = lax.axis_index("sp"), lax.axis_index("tp")
    own_gates = lax.dynamic_index_in_dim(gate_weight, sp, 1, keepdims=False)
    own_gates = jnp.pad(own_gates, ((0, 124), (0, 0)))
    own_bias = lax.dynamic_index_in_dim(gate_bias, sp, 1, keepdims=False)
    own_bias = jnp.pad(own_bias, (0, 124))[None]
    everything, decay, in_weight, out_weight = gather_all(
        tokens[0],
        decay_extra[0].transpose(1, 0, 2),
        (
            query_weight,
            key_weight,
            value_weight,
            outgate_weight,
            pool_weight,
            mem_out_weight,
            pool_out_weight,
        ),
    )
    seq = everything.shape[0]
    decay = decay.transpose(1, 0, 2).reshape(2, 1, seq)
    decay = jnp.pad(decay, ((0, 0), (1, 0), (0, 0))).reshape(4, seq)
    decay = jnp.pad(decay, ((0, 4), (0, 0)))
    proj, pre = project_in(everything, norm_gain, in_weight, own_gates, own_bias)
    memory = lax.dynamic_index_in_dim(init_memory[0], sp, 1, keepdims=False)
    normalizer = lax.dynamic_index_in_dim(init_normalizer[0], sp, 1, keepdims=False)
    gain = lax.dynamic_slice_in_dim(head_gain, sp, 1, 0)
    memory_out = memory_mix(
        proj, pre, decay, memory.reshape(2 * width, width), normalizer, gain, width
    )
    pool_input = proj[:, 4 * width :]
    features = pool_input.shape[1]
    padded = jnp.pad(pool_input.astype(jnp.float32), ((HALO, HALO), (0, 0)))
    positions = jnp.arange(seq, dtype=jnp.int32)
    channels = (tp * n_sp + sp) * features + jnp.arange(features, dtype=jnp.int32)
    pool_out = pool_window(padded, positions, channels, seq, model_width // 4)
    mixed = project_out(memory_out, pool_out, out_weight)
    return mixed[None]


def solution(mesh):
    placed = (
        P("fs", "sp", None),
        P(),
        P(("sp", "fs"), "tp"),
        P(("sp", "fs"), "tp"),
        P(("sp", "fs"), "tp"),
        P(("sp", "fs"), "tp"),
        P(None, "tp", None),
        P(None, "tp"),
        P("fs", None, "tp", "sp"),
        P("fs", None, "tp", None, None),
        P("fs", None, "tp", None),
        P("tp", None),
        P(("sp", "fs"), "tp"),
        P(("sp", "fs"), "tp"),
        P(("sp", "fs"), "tp"),
    )

    def body(*args):
        heads, width = args[11].shape
        features = args[12].shape[1]
        fits = (
            lax.axis_size("tp") == 2
            and heads == lax.axis_size("sp")
            and heads > 1
            and lax.axis_size("fs") == 4
            and heads % 2 == 0
            and width == 128
            and features % (128 * heads) == 0
            and args[0].shape[1] % 32 == 0
        )
        return (by_head if fits else per_device)(*args)

    return jax.shard_map(
        body,
        mesh=mesh,
        in_specs=placed,
        out_specs=P("fs", ("sp", "tp"), None),
        check_vma=False,
    )
```

profile of v0, /device:TPU:0, one launch (start us, length us, event | category | flops | bytes accessed | tf_op | source)
XLA Modules:
  0.0 148.9 jit_solution(16439596497794252155)
XLA Ops:
  0.0 0.0 copy-start
  0.0 0.9 constant_dynamic-slice_fusion.3
  1.0 0.8 pad.20.gates_ref
  1.8 0.9 dynamic-slice_reduce_fusion
  2.7 0.6 pad_bitcast_fusion.bias_ref
  3.2 1.3 copy.24
  4.5 72.3 %gather_all.1 = (bf16[1024,2048]{1,0:T(8,128)(2,1)}, f32[4,2,256]{2,1,0:T(2,128)}, bf16[2048,768]{1,0:T(8,128)(2,1)}, bf16[2048,384]{1,0:T(8,128)(2,1)}) custom-call(bf16[256,2048]{1,0:T(8,128)(2,1)} %bitcast.19, f32[4,2,256]{2,1,0:T(2,128)} %bitcast.22, bf16[128,512]{1,0:T(8,128)(2,1)} %refs_2_.1, bf16[128,512]{1,0:T(8,128)(2,1)} %refs_3_.1, ...), custom_call_target="tpu_custom_call" | custom-call | tf_op jit(solution)/shard_map/gather_all/pallas_call | solution.py:562
  76.8 9.2 %project_in.1 = (bf16[1024,768]{1,0:T(8,128)(2,1)}, f32[1024,128]{1,0:T(8,128)}) custom-call(bf16[1024,2048]{1,0:T(8,128)(2,1)} %get-tuple-element.11.x_ref, f32[1,2048]{1,0:T(1,128)} %bitcast.23, bf16[2048,768]{1,0:T(8,128)(2,1)} %get-tuple-element.12.weight_ref, bf16[128,2048]{1,0:T(8,128)(2,1)} %pad.20.gates_ref, f32[1,128]{1,0:T(1,128)} %pad_bitcast_fusion.bias_ref), custom_call_target="tpu_custom_call" | custom-call | tf_op jit(solution)/shard_map/project_in/pallas_call | solution.py:624
  86.0 0.0 copy-start.3
  86.0 1.1 slice_convert_fusion
  87.3 2.5 %subtract_convert_fusion.pool_ref = bf16[1024,256]{1,0:T(8,128)(2,1)S(1)} fusion(f32[1024,256]{1,0:T(8,128)S(1)} %slice_convert_fusion, s32[256]{0:T(256)S(1)} %get-tuple-element.33, s32[256]{0:T(256)S(1)} %get-tuple-element.34, f32[256]{0:T(256)S(1)} %get-tuple-element.17, f32[256]{0:T(256)S(1)} %get-tuple-element.18, f32[256]{0:T(256)S(1)} %get-tuple-element.19, ...), kind=kLoop, calls=%fused_computation | loop fusion | flops 10747904 | bytes 1591296 | tf_op jit(solution)/shard_map/convert_element_type | solution.py:162
  89.9 0.0 copy-done
  89.9 0.7 constant_dynamic-slice_fusion.2
  90.6 1.2 constant_dynamic-slice_fusion.1
  91.8 1.3 constant_dynamic-slice_fusion.gain_ref
  93.0 0.0 copy-done.3
  93.1 0.6 pad.23.decay_ref
  93.7 0.0 copy-start.1
  93.7 9.1 %memory_mix.1.mem_ref = bf16[1024,128]{1,0:T(8,128)(2,1)} custom-call(bf16[1024,768]{1,0:T(8,128)(2,1)} %get-tuple-element.13.q_ref.qk_ref.k_ref.v_ref.gate_ref, bf16[1024,768]{1,0:T(8,128)(2,1)} %get-tuple-element.13.q_ref.qk_ref.k_ref.v_ref.gate_ref, bf16[1024,768]{1,0:T(8,128)(2,1)} %get-tuple-element.13.q_ref.qk_ref.k_ref.v_ref.gate_ref, ...), custom_call_target="tpu_custom_call" | custom-call | tf_op jit(solution)/shard_map/memory_mix/pallas_call | solution.py:758
  102.8 0.0 copy-done.1
  102.8 0.0 copy-start.2
  102.9 0.9 copy-done.2
  103.8 44.3 %project_out.1 = bf16[128,2048]{1,0:T(8,128)(2,1)S(1)} custom-call(bf16[1024,128]{1,0:T(8,128)(2,1)S(1)} %copy-done.2, bf16[1024,256]{1,0:T(8,128)(2,1)S(1)} %subtract_convert_fusion.pool_ref, bf16[2048,384]{1,0:T(8,128)(2,1)S(1)} %copy-done.1), custom_call_target="tpu_custom_call" | custom-call | tf_op jit(solution)/shard_map/project_out/pallas_call | solution.py:900
  148.2 0.8 copy.26
  (13 shorter events, 0.2 us)
Async XLA Ops:
  0.0 89.9 %copy-start = (f32[1,2,4,128,128]{4,3,2,1,0:T(8,128)S(1)}, f32[1,2,4,128,128]{4,3,2,1,0:T(8,128)}, u32[]{:S(2)}) copy-start(f32[1,2,4,128,128]{4,3,2,1,0:T(8,128)} %param.24) | copy-start | bytes 1572868
  86.0 7.0 %copy-start.3 = (f32[4,2,256]{2,1,0:T(2,128)S(1)}, f32[4,2,256]{2,1,0:T(2,128)}, u32[]{:S(2)}) copy-start(f32[4,2,256]{2,1,0:T(2,128)} %get-tuple-element.15) | copy-start | bytes 24580
  93.7 9.1 %copy-start.1 = (bf16[2048,384]{1,0:T(8,128)(2,1)S(1)}, bf16[2048,384]{1,0:T(8,128)(2,1)}, u32[]{:S(2)}) copy-start(bf16[2048,384]{1,0:T(8,128)(2,1)} %get-tuple-element.16.weight_ref) | copy-start | bytes 4718596
  102.8 1.0 copy-start.2
where the time goes:
time: 149 us
  Pallas kernels  135 us (91%)
  local copies, waits for them, and re-layouts  10.1 us (7%)
  other arithmetic  3.79 us (3%)
    pallas_call x1, Pallas kernels, gather_all(): pl.pallas_call(functools.partial(gather_kernel, n_sp, n_fs, widths), out_...  72.3 us
    pallas_call x1, Pallas kernels, project_out(): pl.pallas_call(functools.partial(project_kernel, n_sp), out_shape=jax.Sha...  44.3 us
    pallas_call x1, Pallas kernels, project_in(): pl.pallas_call(input_kernel, grid=(seq // tb,), out_shape=(jax.ShapeDtype...  9.17 us
    pallas_call x1, Pallas kernels, memory_mix(): pl.pallas_call(memory_kernel, grid=(seq // tb,), out_shape=jax.ShapeDtype...  9.11 us
    unnamed x12, local copies, waits for them, and re-layouts  3.07 us

commit v1 on v0

v1 whole, which is shorter than its diff:
```python
import functools
import math

import jax
import jax.numpy as jnp
from jax import lax
from jax.experimental import pallas as pl
from jax.experimental.pallas import tpu as pltpu
from jax.sharding import PartitionSpec as P

MESH = pl.DeviceIdType.MESH

HALO = 8


norm_eps = 1e-06
exact_mode = lax.Precision.HIGHEST


def carried_in(x, axis, combine, identity, reverse):
    length, position = (lax.axis_size(axis), lax.axis_index(axis))
    everything = jax.tree.map(lambda part: lax.all_gather(part, axis), x)
    start = jax.tree.map(
        lambda part, zero: jnp.broadcast_to(jnp.asarray(zero, part.dtype), part.shape), x, identity
    )

    def lap(k, before):
        at = length - 1 - k if reverse else k
        reached = at > position if reverse else at < position
        new = combine(before, jax.tree.map(lambda part: part[at], everything))
        return jax.tree.map(lambda a, b: jnp.where(reached, a, b), new, before)

    return lax.fori_loop(0, length, lap, start)


def padded_2(block, sides, width):
    for axis, dim in sides:
        count = lax.axis_size(axis)
        forward = [(i, i + 1) for i in range(count - 1)]
        backward = [(target, source) for source, target in forward]
        low = lax.ppermute(
            lax.slice_in_dim(block, block.shape[dim] - width, None, axis=dim), axis, forward
        )
        high = lax.ppermute(lax.slice_in_dim(block, 0, width, axis=dim), axis, backward)
        block = jnp.concatenate([low, block, high], axis=dim)
    return block


def block_output(
    query_rows, key_rows, value_rows, input_gate, log_forget, memory, normalizer, stabilizer
):
    block_len = query_rows.shape[1]
    key_scale = key_rows.shape[-1] ** (-0.5)
    lower_mask = jnp.tril(jnp.ones((block_len, block_len), dtype=bool))
    summed = jnp.cumsum(log_forget, axis=-1)
    log_decay = jnp.where(
        lower_mask, summed[:, :, None] - summed[:, None, :] + input_gate[:, None, :], -jnp.inf
    )
    log_carry = stabilizer[:, None] + summed
    running_max = jnp.maximum(log_carry, jnp.max(log_decay, axis=-1))
    scores = (
        jnp.einsum("btd,bsd->bts", query_rows, key_rows, preferred_element_type=jnp.float32)
        * key_scale
    )
    inner_weight = jnp.exp(log_decay - running_max[:, :, None]) * scores
    weight_rounded = inner_weight.astype(jnp.bfloat16)
    carry_weight = jnp.exp(log_carry - running_max)
    query_wide = query_rows.astype(jnp.float32)
    numerator = carry_weight[:, :, None] * jnp.einsum(
        "bed,btd->bte", memory, query_wide, precision=exact_mode
    )
    numerator = numerator + jnp.einsum(
        "bts,bse->bte", weight_rounded, value_rows, preferred_element_type=jnp.float32
    )
    denominator = carry_weight * jnp.einsum(
        "bd,btd->bt", normalizer, query_wide, precision=exact_mode
    )
    denominator = denominator + jnp.sum(inner_weight, axis=-1)
    return numerator / jnp.maximum(jnp.abs(denominator), jnp.exp(-running_max))[:, :, None]


def block_summary(key_rows, value_rows, input_gate, log_forget):
    key_wide = key_rows.astype(jnp.float32) * key_rows.shape[-1] ** (-0.5)
    summed = jnp.cumsum(log_forget, axis=-1)
    forget_total = summed[:, -1]
    log_weight = forget_total[:, None] - summed + input_gate
    running_max = jnp.max(log_weight, axis=-1)
    weights = jnp.exp(log_weight - running_max[:, None])
    memory = jnp.einsum(
        "bse,bsd->bed",
        weights[:, :, None] * value_rows.astype(jnp.float32),
        key_wide,
        precision=exact_mode,
    )
    normalizer = jnp.einsum("bs,bsd->bd", weights, key_wide, precision=exact_mode)
    return (memory, normalizer, running_max, forget_total)


def combine(earlier, latter):
    early_memory, early_norm, early_max, early_total = earlier
    late_memory, late_norm, late_max, late_total = latter
    joint_max = jnp.maximum(early_max + late_total, late_max)
    early_scale = jnp.exp(early_max + late_total - joint_max)
    late_scale = jnp.exp(late_max - joint_max)
    memory = early_scale[:, None, None] * early_memory + late_scale[:, None, None] * late_memory
    normalizer = early_scale[:, None] * early_norm + late_scale[:, None] * late_norm
    return (memory, normalizer, joint_max, early_total + late_total)


def span_sweep(
    query_rows, key_rows, value_rows, input_gate, log_forget, memory, normalizer, stabilizer, span
):
    block_count = query_rows.shape[1] // span

    def to_blocks(array):
        shaped = array.reshape((array.shape[0], block_count, span) + array.shape[2:])
        return jnp.moveaxis(shaped, 1, 0)

    def advance(carried, pieces):
        query_blk, key_blk, value_blk, gate_blk, forget_blk = pieces
        result = block_output(
            query_blk, key_blk, value_blk, gate_blk, forget_blk, carried[0], carried[1], carried[2]
        )
        return (combine(carried, block_summary(key_blk, value_blk, gate_blk, forget_blk)), result)

    initial = (memory, normalizer, stabilizer, jnp.zeros_like(stabilizer))
    ignored, outputs = lax.scan(
        advance,
        initial,
        tuple(
            (
                to_blocks(array)
                for array in (query_rows, key_rows, value_rows, input_gate, log_forget)
            )
        ),
    )
    return jnp.moveaxis(outputs, 0, 1).reshape(query_rows.shape[:2] + (value_rows.shape[2],))


def reverse_time(array):
    return jnp.flip(array, axis=1)


def to_heads(matrix, head_count):
    shaped = matrix.reshape(matrix.shape[0], head_count, matrix.shape[1] // head_count)
    return shaped.transpose(1, 0, 2)


def pool_window(padded, positions, channels, seq_len, group_size):
    row_count = positions.shape[0]
    group_index = channels // group_size
    reach_left = jnp.left_shift(jnp.ones_like(group_index), group_index)
    reach_right = reach_left - 1
    window_sum = jnp.zeros((row_count, channels.shape[0]), jnp.float32)
    for offset in range(-HALO, HALO):
        inside = ((offset >= -reach_left) & (offset <= reach_right)).astype(jnp.float32)
        window_sum = window_sum + inside * padded[HALO + offset : HALO + offset + row_count]
    first_pos = jnp.maximum(positions[:, None] - reach_left[None, :], 0)
    last_pos = jnp.minimum(positions[:, None] + reach_right[None, :], seq_len - 1)
    counted = (last_pos - first_pos + 1).astype(jnp.float32)
    centre = padded[HALO : HALO + row_count]
    return (window_sum / counted - centre).astype(jnp.bfloat16)


def per_device(
    tokens,
    norm_gain,
    query_weight,
    key_weight,
    value_weight,
    outgate_weight,
    gate_weight,
    gate_bias,
    decay_extra,
    init_memory,
    init_normalizer,
    head_gain,
    pool_weight,
    mem_out_weight,
    pool_out_weight,
):
    block_len = tokens.shape[1]
    model_width = tokens.shape[2]
    head_count, head_width = head_gain.shape
    span = math.gcd(block_len, 256)
    flattened = tokens[0].astype(jnp.float32)
    normed = (
        flattened
        * lax.rsqrt(jnp.mean(flattened * flattened, axis=-1, keepdims=True) + norm_eps)
        * norm_gain
    ).astype(jnp.bfloat16)
    zero_start = tuple(
        (
            jnp.zeros((block_len, weight.shape[1]), jnp.float32)
            for weight in (query_weight, key_weight, value_weight, outgate_weight, pool_weight)
        )
    )
    zero_start = zero_start + (
        jnp.zeros((model_width, mem_out_weight.shape[1]), jnp.bfloat16),
        jnp.zeros((model_width, pool_out_weight.shape[1]), jnp.bfloat16),
    )
    line_query, line_key, line_value, line_outgate, line_pool, line_mem_out, line_pool_out = (
        lax.all_gather(query_weight, "fs", axis=0, tiled=True),
        lax.all_gather(key_weight, "fs", axis=0, tiled=True),
        lax.all_gather(value_weight, "fs", axis=0, tiled=True),
        lax.all_gather(outgate_weight, "fs", axis=0, tiled=True),
        lax.all_gather(pool_weight, "fs", axis=0, tiled=True),
        lax.all_gather(mem_out_weight, "fs", axis=0, tiled=True),
        lax.all_gather(pool_out_weight, "fs", axis=0, tiled=True),
    )
    pieces = (
        lax.all_gather(line_query, "sp", axis=0, tiled=True),
        lax.all_gather(line_key, "sp", axis=0, tiled=True),
        lax.all_gather(line_value, "sp", axis=0, tiled=True),
        lax.all_gather(line_outgate, "sp", axis=0, tiled=True),
        lax.all_gather(line_pool, "sp", axis=0, tiled=True),
        lax.all_gather(line_mem_out, "sp", axis=0, tiled=True),
        lax.all_gather(line_pool_out, "sp", axis=0, tiled=True),
    )
    partial_sums = tuple(
        (
            jnp.dot(normed, weight_rows, preferred_element_type=jnp.float32)
            for weight_rows in pieces[:5]
        )
    )
    collected = tuple((weight_rows for weight_rows in pieces[5:]))
    folded = partial_sums + collected
    query_proj, key_proj, value_proj, outgate, pool_input = tuple(
        (running.astype(jnp.bfloat16) for running in folded[:5])
    )
    mem_weight_all = folded[5]
    pool_weight_all = folded[6]
    gate_pre = lax.dot_general(
        normed,
        gate_weight.reshape(4 * head_count, model_width),
        (((1,), (1,)), ((), ())),
        preferred_element_type=jnp.float32,
    ) + gate_bias.reshape(4 * head_count)
    gate_pre = gate_pre.reshape(block_len, 4, head_count).transpose(1, 2, 0)
    query_heads = to_heads(query_proj, head_count)
    key_heads = to_heads(key_proj, head_count)
    value_heads = to_heads(value_proj, head_count)
    forward_forget = jax.nn.log_sigmoid(gate_pre[1]) + decay_extra[0, 0]
    backward_forget = jax.nn.log_sigmoid(gate_pre[3]) + decay_extra[0, 1]
    zero_rows = jnp.zeros((head_count,), jnp.float32)
    identity = (
        jnp.zeros((head_count, head_width, head_width), jnp.float32),
        jnp.zeros((head_count, head_width), jnp.float32),
        jnp.full((head_count,), -1e30, jnp.float32),
        zero_rows,
    )
    front_memory, front_norm, front_max, front_total = block_summary(
        key_heads, value_heads, gate_pre[0], forward_forget
    )
    prefix = carried_in(
        (front_memory, front_norm, front_max, front_total), "sp", combine, identity, False
    )
    incoming = combine((init_memory[0, 0], init_normalizer[0, 0], zero_rows, zero_rows), prefix)
    forward_out = span_sweep(
        query_heads,
        key_heads,
        value_heads,
        gate_pre[0],
        forward_forget,
        incoming[0],
        incoming[1],
        incoming[2],
        span,
    )
    back_query = reverse_time(query_heads)
    back_key = reverse_time(key_heads)
    back_value = reverse_time(value_heads)
    back_gate = reverse_time(gate_pre[2])
    back_forget = reverse_time(backward_forget)
    rear_memory, rear_norm, rear_max, rear_total = block_summary(
        back_key, back_value, back_gate, back_forget
    )
    suffix = carried_in(
        (rear_memory, rear_norm, rear_max, rear_total), "sp", combine, identity, True
    )
    back_incoming = combine(
        (init_memory[0, 1], init_normalizer[0, 1], zero_rows, zero_rows), suffix
    )
    backward_out = reverse_time(
        span_sweep(
            back_query,
            back_key,
            back_value,
            back_gate,
            back_forget,
            back_incoming[0],
            back_incoming[1],
            back_incoming[2],
            span,
        )
    )
    summed_dirs = (forward_out + backward_out).transpose(1, 0, 2)
    normed_heads = (
        summed_dirs
        * lax.rsqrt(jnp.mean(summed_dirs * summed_dirs, axis=-1, keepdims=True) + norm_eps)
        * head_gain
    )
    out_gate = jax.nn.sigmoid(
        outgate.astype(jnp.float32).reshape(block_len, head_count, head_width)
    )
    memory_out = (
        (normed_heads * out_gate).astype(jnp.bfloat16).reshape(block_len, head_count * head_width)
    )
    padded = padded_2(pool_input, (("sp", 0),), HALO).astype(jnp.float32)
    feature_count = pool_input.shape[1]
    positions = lax.axis_index("sp") * block_len + jnp.arange(block_len, dtype=jnp.int32)
    channels = lax.axis_index("tp") * feature_count + jnp.arange(feature_count, dtype=jnp.int32)
    pool_out = pool_window(
        padded, positions, channels, block_len * lax.axis_size("sp"), model_width // 4
    )
    own_rows = block_len // lax.axis_size("tp")
    result = lax.dot_general(
        memory_out, mem_weight_all, (((1,), (1,)), ((), ())), preferred_element_type=jnp.float32
    )
    mixed = lax.psum_scatter(
        (
            result
            + lax.dot_general(
                pool_out,
                pool_weight_all,
                (((1,), (1,)), ((), ())),
                preferred_element_type=jnp.float32,
            )
        ).astype(jnp.bfloat16),
        "tp",
        scatter_dimension=0,
        tiled=True,
    )
    return mixed.reshape(1, own_rows, model_width)


LOG2E = math.log2(math.e)


def scan_lanes(x, combine_, fill, reverse):
    length = x.shape[1]
    lane = lax.broadcasted_iota(jnp.int32, x.shape, 1)
    d = 1
    while d < length:
        if reverse:
            moved = jnp.where(lane < length - d, pltpu.roll(x, length - d, 1), fill)
        else:
            moved = jnp.where(lane >= d, pltpu.roll(x, d, 1), fill)
        x = combine_(x, moved)
        d *= 2
    return x


def transposed_dot(a, b):
    return lax.dot_general(a, b, (((1,), (1,)), ((), ())), preferred_element_type=jnp.float32)


def layer_kernel(
    n_sp,
    token_ref, gain_ref, qw, kw, vw, ow, gate_ref, bias_ref, decay_ref, mem_ref, nrm_ref,
    hgain_ref, pw, mw, fw,
    o_ref,
    x_all, normed, w_all, stage, transit, gmat, dec, init, nrm, proj_a, proj_b, pool_buf, act,
    flat, cols, level_rows, msg_out, msg_in, state_out, state_in, halo_out, halo_in,
    give, take, total, s1, l1, s2, l2,
    loc_w, loc_s, x_ss, x_rs, p_ss, p_rs, h_ss, h_rs, y_ss, y_rs,
    tz_ss, tz_rs, tx_ss, tx_rs, tw_ss, tw_rs, d_ss, d_rs, i_ss, i_rs, m_ss, m_rs,
    sw_ss, sw_rs, r1_ss, r1_rs, r2_ss, r2_rs,
):
    block, width = token_ref.shape
    rows = qw.shape[0]
    hw = hgain_ref.shape[1]
    feat = pw.shape[1] // 4
    half = block // 2
    span = 2 * block
    pieces_t = 2
    part = half // pieces_t
    z, fs, c = lax.axis_index("sp"), lax.axis_index("fs"), lax.axis_index("tp")
    y, x = fs // 2, lax.rem(fs, 2)
    h, p = z // 2, lax.rem(z, 2)
    zn = z + 1 - 2 * p
    zf = lax.rem(z + 2, n_sp)
    zfn = zf + 1 - 2 * p
    xn, yn = 2 * y + 1 - x, 2 * (1 - y) + x
    other = 1 - c
    low = h == 0
    quarter = 2 * p + x
    to_x, to_y, to_p, to_h, to_c = {"fs": xn}, {"fs": yn}, {"sp": zn}, {"sp": zf}, {"tp": other}

    def remote(src, dst, ss, rs, device):
        return pltpu.make_async_remote_copy(
            src_ref=src, dst_ref=dst, send_sem=ss, recv_sem=rs,
            device_id=device, device_id_type=MESH,
        )

    def at(start, size):
        return pl.ds(pl.multiple_of(start, size), size)

    barrier = pltpu.get_barrier_semaphore()
    for device in (to_x, to_y, to_p, to_h, to_c):
        pl.semaphore_signal(barrier, inc=1, device_id=device, device_id_type=MESH)

    groups = (((qw, hw), (kw, hw), (vw, hw)), ((ow, hw), (pw, feat)), ((mw, hw), (fw, feat)))
    quarters = (quarter, 2 * p + 1 - x, 2 * (1 - p) + 1 - x, 2 * (1 - p) + x)

    def row_block(zs, ys, xs):
        return at((zs * 4 + ys * 2 + xs) * rows, rows)

    def local_weights(g):
        copies = []
        for slot in (1, 2, 3, 0):
            start = 0
            for i, (ref, size) in enumerate(groups[g]):
                columns = pl.ds(start, size)
                if slot:
                    dst = stage.at[g, slot - 1, :, columns]
                else:
                    dst = w_all.at[g, row_block(z, y, x), columns]
                copies.append(
                    pltpu.make_async_copy(
                        ref.at[:, at(quarters[slot] * size, size)], dst, loc_w.at[g, slot, i]
                    )
                )
                start += size
        return copies

    locals_ = [local_weights(g) for g in range(3)]
    own_tokens = pltpu.make_async_copy(
        token_ref, x_all.at[at((2 * x + p) * block, block)], loc_s.at[0]
    )
    own_decay = pltpu.make_async_copy(decay_ref, dec.at[x, p], loc_s.at[1])
    own_init = pltpu.make_async_copy(mem_ref.at[h, quarter], init.at[x], loc_s.at[2])
    own_nrm = pltpu.make_async_copy(nrm_ref, nrm.at[x], loc_s.at[3])
    for copy in locals_[0]:
        copy.start()
    own_tokens.start()
    for copy in locals_[1] + locals_[2]:
        copy.start()
    for copy in (own_decay, own_init, own_nrm):
        copy.start()

    def x_copy(g, s, incoming=False):
        if s == 0:
            dst = w_all.at[g, row_block(z, y, 1 - x if incoming else x)]
        else:
            dst = transit.at[g]
        return remote(dst if incoming else stage.at[g, s], dst, x_ss.at[g, s], x_rs.at[g, s], to_x)

    def p_copy(g, s, incoming=False):
        dst = w_all.at[g, row_block(zn if incoming else z, y, 1 - x if s else x)]
        src = dst if incoming else (transit.at[g] if s else stage.at[g, 2])
        return remote(src, dst, p_ss.at[g, s], p_rs.at[g, s], to_p)

    def h_copy(g, k, s, incoming=False):
        source = (zf, zfn)[k] if incoming else (z, zn)[k]
        ref = w_all.at[g, row_block(source, y, 1 - x if s else x)]
        return remote(ref, ref, h_ss.at[g, k, s], h_rs.at[g, k, s], to_h)

    def y_copy(g, k, s, incoming=False):
        ref = w_all.at[
            g, row_block((z, zn, zf, zfn)[k], 1 - y if incoming else y, 1 - x if s else x)
        ]
        return remote(ref, ref, y_ss.at[g, k, s], y_rs.at[g, k, s], to_y)

    sent = []

    def go(copy):
        copy.start()
        sent.append(copy)

    def begin(g):
        for copy in locals_[g]:
            copy.wait()
        go(x_copy(g, 1))
        go(x_copy(g, 0))
        go(p_copy(g, 0))
        go(h_copy(g, 0, 0))
        go(y_copy(g, 0, 0))

    def after_x(g):
        x_copy(g, 1, True).wait_recv()
        go(p_copy(g, 1))
        x_copy(g, 0, True).wait_recv()
        go(h_copy(g, 0, 1))
        go(y_copy(g, 0, 1))

    def after_p(g):
        for s in range(2):
            p_copy(g, s, True).wait_recv()
            go(h_copy(g, 1, s))
            go(y_copy(g, 1, s))

    def after_h(g):
        for k in range(2):
            for s in range(2):
                h_copy(g, k, s, True).wait_recv()
                go(y_copy(g, 2 + k, s))

    def after_y(g):
        for k in range(4):
            for s in range(2):
                y_copy(g, k, s, True).wait_recv()

    def token_rows(j, b, side, i):
        return at((2 * j + b) * block + side * half + i * part, part)

    def token_p(i, incoming=False):
        b = 1 - p if incoming else p
        dst = x_all.at[token_rows(x, b, c, i)]
        src = dst if incoming else token_ref.at[at(c * half + i * part, part)]
        return remote(src, dst, tz_ss.at[i], tz_rs.at[i], to_p)

    def token_x(kind, i, incoming=False):
        b = 1 - p if kind else p
        dst = x_all.at[token_rows(1 - x if incoming else x, b, c, i)]
        src = dst if incoming or kind else token_ref.at[at(c * half + i * part, part)]
        return remote(src, dst, tx_ss.at[kind, i], tx_rs.at[kind, i], to_x)

    places = ((x, 1 - p), (1 - x, p), (1 - x, 1 - p))

    def token_swap(which, i, incoming=False):
        j, b = places[which]
        ref = x_all.at[token_rows(j, b, other if incoming else c, i)]
        return remote(ref, ref, tw_ss.at[which, i], tw_rs.at[which, i], to_c)

    def decay_p(incoming=False):
        dst = dec.at[x, 1 - p if incoming else p]
        return remote(dst if incoming else decay_ref, dst, d_ss.at[0], d_rs.at[0], to_p)

    def decay_x(kind, incoming=False):
        dst = dec.at[1 - x if incoming else x, 1 - p if kind else p]
        src = dst if incoming or kind else decay_ref
        return remote(src, dst, d_ss.at[1 + kind], d_rs.at[1 + kind], to_x)

    def init_x(which, incoming=False):
        dst = (init, nrm)[which].at[1 - x if incoming else x]
        src = (mem_ref.at[h, 2 * p + 1 - x], nrm_ref)[which]
        return remote(dst if incoming else src, dst, i_ss.at[which], i_rs.at[which], to_x)

    def normalise(j, b):
        step = 64

        def body(i, carry):
            here = at((2 * j + b) * block + i * step, step)
            wide = x_all[here, :].astype(jnp.float32)
            normed[here, :] = (
                wide
                * lax.rsqrt(jnp.mean(wide * wide, axis=-1, keepdims=True) + norm_eps)
                * gain_ref[...]
            ).astype(jnp.bfloat16)
            return carry

        lax.fori_loop(0, block // step, body, 0)

    pl.semaphore_wait(barrier, 5)
    begin(0)
    for i in range(pieces_t):
        go(token_p(i))
        go(token_x(0, i))
    own_decay.wait()
    go(decay_p())
    go(decay_x(0))
    gmat[...] = jnp.zeros_like(gmat)
    pick = lax.broadcasted_iota(jnp.int32, (4, width), 0) == quarter
    row16 = lax.broadcasted_iota(jnp.int32, (16, width), 0)
    gates16 = jnp.zeros((16, width), jnp.float32)
    for i in range(4):
        row = jnp.sum(
            jnp.where(pick, gate_ref[i].astype(jnp.float32), 0.0), axis=0, keepdims=True
        )
        gates16 = jnp.where((row16 == i) | (row16 == i + 4), row, gates16)
    gmat[0:16, :] = gates16.astype(jnp.bfloat16)
    own_tokens.wait()
    normalise(x, p)
    after_x(0)
    begin(1)
    go(init_x(0))
    go(init_x(1))
    for i in range(pieces_t):
        token_p(i, True).wait_recv()
        go(token_swap(0, i))
        go(token_x(1, i))
    decay_p(True).wait_recv()
    go(decay_x(1))
    after_p(0)
    for i in range(pieces_t):
        token_x(0, i, True).wait_recv()
        go(token_swap(1, i))
    for i in range(pieces_t):
        token_swap(0, i, True).wait_recv()
    normalise(x, 1 - p)
    after_x(1)
    begin(2)
    for i in range(pieces_t):
        token_swap(1, i, True).wait_recv()
    normalise(1 - x, p)
    after_h(0)
    for i in range(pieces_t):
        token_x(1, i, True).wait_recv()
        go(token_swap(2, i))
    after_p(1)
    for i in range(pieces_t):
        token_swap(2, i, True).wait_recv()
    normalise(1 - x, 1 - p)
    decay_x(0, True).wait_recv()
    decay_x(1, True).wait_recv()

    tall = []
    for j in range(2):
        pieces = []
        for b in range(2):
            pre = transposed_dot(normed[(2 * j + b) * block : (2 * j + b + 1) * block, :], gmat[...])
            pieces.append(pre.T[:8])
        tall.append(jnp.concatenate(pieces, axis=1))
    row8 = lax.broadcasted_iota(jnp.int32, (8, span), 0)
    gates = jnp.where(row8 < 4, tall[0], tall[1])
    extra = jnp.zeros((8, span), jnp.float32)
    for i in range(4):
        gates = gates + jnp.where((row8 == i) | (row8 == i + 4), bias_ref[i, quarter], 0.0)
    for j in range(2):
        for direction in range(2):
            value = jnp.concatenate(
                [dec[j, b, direction, pl.ds(quarter, 1), :] for b in range(2)], axis=1
            )
            extra = jnp.where(row8 == 4 * j + 1 + 2 * direction, value, extra)
    forget = jnp.minimum(gates, 0.0) - jnp.log1p(jnp.exp(-jnp.abs(gates))) + extra
    sum_f = pltpu.roll(scan_lanes(forget, jnp.add, 0.0, False), 7, 0)
    sum_b = pltpu.roll(scan_lanes(forget, jnp.add, 0.0, True), 7, 0)
    level_f = gates - sum_f
    level_b = gates - sum_b
    run_f = scan_lanes(level_f, jnp.maximum, -1e30, False)
    run_b = scan_lanes(level_b, jnp.maximum, -1e30, True)
    top_f = jnp.maximum(run_f[:, span - 1 : span], 0.0)
    top_b = jnp.maximum(run_b[:, 0:1], 0.0)
    end_f = sum_f[:, span - 1 : span] + top_f
    end_b = sum_b[:, 0:1] + top_b
    msg_out[...] = jnp.broadcast_to(jnp.where(low, end_f, end_b), msg_out.shape)

    def message(which, incoming=False):
        src = (msg_out, state_out, halo_out)[which]
        dst = (msg_in, state_in, halo_in)[which]
        return remote(dst if incoming else src, dst, m_ss.at[which], m_rs.at[which], to_h)

    go(message(0))

    after_y(0)

    def project(g, store):
        def body(i, carry):
            here = at(i * block, block)
            store(i, jnp.dot(
                normed[here, :], w_all[g], preferred_element_type=jnp.float32
            ).astype(jnp.bfloat16))
            return carry

        lax.fori_loop(0, 4, body, 0)

    def store_a(i, value):
        proj_a[at(i * block, block), :] = value

    project(0, store_a)
    after_h(1)

    message(0, True).wait_recv()
    arrived = msg_in[:, 0:1]
    enter_f = jnp.where(low, 0.0, arrived)
    enter_b = jnp.where(low, arrived, 0.0)
    scale_bits = -0.5 * math.log2(hw)
    lf2 = level_f * LOG2E + scale_bits
    lb2 = level_b * LOG2E + scale_bits
    peak_f = jnp.maximum(run_f, enter_f)
    peak_b = jnp.maximum(run_b, enter_b)
    level_rows[0:8, :] = lf2
    level_rows[8:16, :] = lb2
    flat[48:, :] = jnp.zeros_like(flat[48:, :])
    flat[0:8, :] = peak_f * LOG2E
    flat[8:16, :] = peak_b * LOG2E
    flat[16:24, :] = jnp.exp(enter_f - peak_f)
    flat[24:32, :] = jnp.exp(enter_b - peak_b)
    flat[32:40, :] = jnp.exp(-(sum_f + peak_f))
    flat[40:48, :] = jnp.exp(-(sum_b + peak_b))
    cols[...] = flat[...].T

    own_init.wait()
    own_nrm.wait()
    init_x(0, True).wait_recv()
    init_x(1, True).wait_recv()
    leave_f = jnp.exp2(lf2 - top_f * LOG2E)
    leave_b = jnp.exp2(lb2 - top_b * LOG2E)
    keep_f = jnp.exp(-top_f)
    keep_b = jnp.exp(-top_b)
    starts = []
    for j in range(2):
        here = slice(j * span, (j + 1) * span)
        own = jnp.where(low, leave_f[4 * j : 4 * j + 1], leave_b[4 * j + 2 : 4 * j + 3])
        kept = jnp.where(low, keep_f[4 * j : 4 * j + 1], keep_b[4 * j + 2 : 4 * j + 3])
        values = proj_a[here, 2 * hw : 3 * hw].astype(jnp.float32).T * own
        lhs = jnp.concatenate(
            [values, jnp.broadcast_to(own, (8, span))], axis=0
        ).astype(jnp.bfloat16)
        grown = jnp.dot(lhs, proj_a[here, hw : 2 * hw], preferred_element_type=jnp.float32)
        start = jnp.concatenate(
            [init[j], jnp.broadcast_to(nrm[j, h, pl.ds(quarter, 1), :], (8, hw))], axis=0
        )
        starts.append(start)
        state_out[j] = kept * start + grown
    go(message(1))

    after_y(1)

    def store_b(i, value):
        proj_b[at(i * block, block), :] = value[:, :hw]
        pool_buf[i // 2, pl.ds(pl.multiple_of(8 + lax.rem(i, 2) * block, 8), block), :] = value[
            :, hw:
        ].astype(jnp.float32)

    project(1, store_b)
    for j in range(2):
        halo_out[j] = jnp.where(low, pool_buf[j, span : span + 8, :], pool_buf[j, 8:16, :])
    go(message(2))
    after_x(2)
    after_p(2)

    message(1, True).wait_recv()
    for j in range(2):
        here = slice(j * span, (j + 1) * span)
        front_start = jnp.where(low, starts[j], state_in[j])
        rear_start = jnp.where(low, state_in[j], starts[j])
        carry_in = jnp.concatenate(
            [front_start[:hw], rear_start[:hw], front_start[hw:], rear_start[hw:]], axis=0
        )
        carry_in = jnp.concatenate(
            [carry_in, jnp.zeros((3 * hw - carry_in.shape[0], hw), jnp.float32)], axis=0
        )
        coarse = carry_in.astype(jnp.bfloat16)
        fine = (carry_in - coarse.astype(jnp.float32)).astype(jnp.bfloat16)
        for i in range(4):
            r0 = i * half
            mine = slice(j * span + r0, j * span + r0 + half)
            q = proj_a[mine, 0:hw]
            carry = transposed_dot(q, coarse) + transposed_dot(q, fine)
            score = transposed_dot(q, proj_a[here, hw : 2 * hw])
            col = cols[r0 : r0 + half, :]

            def direction(first, last, level, peak, decay, floor, got, den0, rear):
                weight = jnp.exp2(level[:, first:last] - peak) * score[:, first:last]
                t = r0 + lax.broadcasted_iota(jnp.int32, weight.shape, 0)
                s = first + lax.broadcasted_iota(jnp.int32, weight.shape, 1)
                weight = jnp.where(s >= t if rear else s <= t, weight, 0.0)
                num = decay * got + jnp.dot(
                    weight.astype(jnp.bfloat16),
                    proj_a[j * span + first : j * span + last, 2 * hw : 3 * hw],
                    preferred_element_type=jnp.float32,
                )
                den = decay * den0 + jnp.sum(weight, axis=1, keepdims=True)
                return num / jnp.maximum(jnp.abs(den), floor)

            f, b = 4 * j, 4 * j + 2
            summed = direction(
                0, r0 + half, level_rows[f : f + 1, :], col[:, f : f + 1],
                col[:, 16 + f : 17 + f], col[:, 32 + f : 33 + f],
                carry[:, :hw], carry[:, 2 * hw : 2 * hw + 1], False,
            ) + direction(
                r0, span, level_rows[8 + b : 9 + b, :], col[:, 8 + b : 9 + b],
                col[:, 24 + b : 25 + b], col[:, 40 + b : 41 + b],
                carry[:, hw : 2 * hw], carry[:, 2 * hw + 8 : 2 * hw + 9], True,
            )
            out = (
                summed
                * lax.rsqrt(jnp.mean(summed * summed, axis=-1, keepdims=True) + norm_eps)
                * hgain_ref[pl.ds(quarter, 1), :]
                * jax.nn.sigmoid(proj_b[mine, :].astype(jnp.float32))
            )
            place = (i % 2) * span + (2 * j + i // 2) * half
            act[place : place + half, 0:hw] = out.astype(jnp.bfloat16)
        if j == 0:
            after_h(2)

    message(2, True).wait_recv()
    for j in range(2):
        zero = jnp.zeros((8, feat), jnp.float32)
        pool_buf[j, 0:8, :] = jnp.where(low, zero, halo_in[j])
        pool_buf[j, span + 8 : span + 16, :] = jnp.where(low, halo_in[j], zero)
    group = (c * 4 + quarter) * feat * 4 // width
    for k in range(4):

        @pl.when(group == k)
        def _(k=k):
            reach = 2 ** k
            t = h * span + lax.broadcasted_iota(jnp.int32, (span, 1), 0)
            counted = jnp.minimum(t + reach - 1, n_sp * block - 1) - jnp.maximum(t - reach, 0) + 1
            counted = counted.astype(jnp.float32)
            length = span + 16
            for j in range(2):
                window = pool_buf[j]
                for e in range(k + 1):
                    window = window + pltpu.roll(window, length - 2 ** e, 0)
                if reach < 8:
                    window = pltpu.roll(window, length - (8 - reach), 0)
                value = window[:span] / counted - pool_buf[j, 8 : 8 + span, :]
                value = value.astype(jnp.bfloat16)
                for i in range(4):
                    place = (i % 2) * span + (2 * j + i // 2) * half
                    act[place : place + half, hw:] = value[i * half : (i + 1) * half]

    after_y(2)
    count = give.shape[0]
    tile = width // count

    def swap(n):
        return remote(give.at[n], take.at[n], sw_ss.at[n], sw_rs.at[n], to_c)

    def first_stage(n, slot, incoming=False):
        dst = l1.at[n, slot]
        return remote(
            dst if incoming else s1.at[n, slot], dst, r1_ss.at[n, slot], r1_rs.at[n, slot],
            to_p if n % 2 else to_x,
        )

    def second_stage(n, incoming=False):
        return remote(
            l2.at[n] if incoming else s2.at[n], l2.at[n], r2_ss.at[n], r2_rs.at[n],
            to_x if n % 2 else to_p,
        )

    def product(side, n):
        return transposed_dot(act[at(side * span, span), :], w_all[2, n * tile : (n + 1) * tile, :])

    for n in range(count):
        give[n] = product(other, n).astype(jnp.bfloat16).reshape(give.shape[1:])
        go(swap(n))
    home = 2 * x + p
    both = 2 * (1 - x) + 1 - p
    for n in range(count):
        part_sum = product(c, n)
        swap(n).wait_recv()
        total[n] = part_sum.reshape(total.shape[1:]) + take[n].astype(jnp.float32)
        near, middle = 2 * (1 - x) + p, 2 * x + 1 - p
        if n % 2:
            near, middle = middle, near
        s1[n, 1] = total[n, both].astype(jnp.bfloat16)
        go(first_stage(n, 1))
        s1[n, 0] = total[n, near].astype(jnp.bfloat16)
        go(first_stage(n, 0))
    for n in range(count):
        middle = 2 * (1 - x) + p if n % 2 else 2 * x + 1 - p
        first_stage(n, 1, True).wait_recv()
        s2[n] = (total[n, middle] + l1[n, 1].astype(jnp.float32)).astype(jnp.bfloat16)
        go(second_stage(n))
    for n in range(count):
        first_stage(n, 0, True).wait_recv()
        second_stage(n, True).wait_recv()
        o_ref[:, n * tile : (n + 1) * tile] = (
            total[n, home] + l1[n, 0].astype(jnp.float32) + l2[n].astype(jnp.float32)
        ).astype(jnp.bfloat16)
    for copy in sent:
        copy.wait_send()


def by_group(
    tokens, norm_gain, query_weight, key_weight, value_weight, outgate_weight, gate_weight,
    gate_bias, decay_extra, init_memory, init_normalizer, head_gain, pool_weight, mem_out_weight,
    pool_out_weight,
):
    n_sp = lax.axis_size("sp")
    block, width = tokens.shape[1:]
    rows = query_weight.shape[0]
    hw = head_gain.shape[1]
    feat = pool_weight.shape[1] // 4
    columns = 3 * hw
    half, span, everything = block // 2, 2 * block, 4 * block
    count = 4
    tile = width // count
    f32, bf16 = jnp.float32, jnp.bfloat16
    dma = pltpu.SemaphoreType.DMA
    vmem = pl.BlockSpec(memory_space=pltpu.VMEM)
    anywhere = pl.BlockSpec(memory_space=pl.ANY)
    smem = pl.BlockSpec(memory_space=pltpu.SMEM)
    mixed = pl.pallas_call(
        functools.partial(layer_kernel, n_sp),
        out_shape=jax.ShapeDtypeStruct((half, width), bf16),
        in_specs=[
            anywhere, vmem, anywhere, anywhere, anywhere, anywhere, vmem, smem, anywhere, anywhere,
            anywhere, vmem, anywhere, anywhere, anywhere,
        ],
        out_specs=vmem,
        scratch_shapes=[
            pltpu.VMEM((everything, width), bf16),
            pltpu.VMEM((everything, width), bf16),
            pltpu.VMEM((3, width, columns), bf16),
            pltpu.VMEM((3, 3, rows, columns), bf16),
            pltpu.VMEM((3, rows, columns), bf16),
            pltpu.VMEM((128, width), bf16),
            pltpu.VMEM((2, 2) + decay_extra.shape[1:], f32),
            pltpu.VMEM((2, hw, hw), f32),
            pltpu.VMEM((2,) + init_normalizer.shape[1:], f32),
            pltpu.VMEM((everything, columns), bf16),
            pltpu.VMEM((everything, hw), bf16),
            pltpu.VMEM((2, span + 16, feat), f32),
            pltpu.VMEM((everything, columns), bf16),
            pltpu.VMEM((128, span), f32),
            pltpu.VMEM((span, 128), f32),
            pltpu.VMEM((16, span), f32),
            pltpu.VMEM((8, 128), f32),
            pltpu.VMEM((8, 128), f32),
            pltpu.VMEM((2, hw + 8, hw), f32),
            pltpu.VMEM((2, hw + 8, hw), f32),
            pltpu.VMEM((2, 8, feat), f32),
            pltpu.VMEM((2, 8, feat), f32),
            pltpu.VMEM((count, 4, half, tile), bf16),
            pltpu.VMEM((count, 4, half, tile), bf16),
            pltpu.VMEM((count, 4, half, tile), f32),
            pltpu.VMEM((count, 2, half, tile), bf16),
            pltpu.VMEM((count, 2, half, tile), bf16),
            pltpu.VMEM((count, half, tile), bf16),
            pltpu.VMEM((count, half, tile), bf16),
            dma((3, 4, 3)),
            dma((4,)),
            dma((3, 2)), dma((3, 2)),
            dma((3, 2)), dma((3, 2)),
            dma((3, 2, 2)), dma((3, 2, 2)),
            dma((3, 4, 2)), dma((3, 4, 2)),
            dma((2,)), dma((2,)),
            dma((2, 2)), dma((2, 2)),
            dma((3, 2)), dma((3, 2)),
            dma((3,)), dma((3,)),
            dma((2,)), dma((2,)),
            dma((3,)), dma((3,)),
            dma((count,)), dma((count,)),
            dma((count, 2)), dma((count, 2)),
            dma((count,)), dma((count,)),
        ],
        compiler_params=pltpu.CompilerParams(
            collective_id=0, has_side_effects=True, vmem_limit_bytes=60 * 2**20
        ),
        name="layer",
    )(
        tokens[0], norm_gain[None], query_weight, key_weight, value_weight, outgate_weight,
        gate_weight, gate_bias, decay_extra[0], init_memory[0], init_normalizer[0], head_gain,
        pool_weight, mem_out_weight, pool_out_weight,
    )
    return mixed[None]


def solution(mesh):
    placed = (
        P("fs", "sp", None),
        P(),
        P(("sp", "fs"), "tp"),
        P(("sp", "fs"), "tp"),
        P(("sp", "fs"), "tp"),
        P(("sp", "fs"), "tp"),
        P(None, "tp", None),
        P(None, "tp"),
        P("fs", None, "tp", "sp"),
        P("fs", None, "tp", None, None),
        P("fs", None, "tp", None),
        P("tp", None),
        P(("sp", "fs"), "tp"),
        P(("sp", "fs"), "tp"),
        P(("sp", "fs"), "tp"),
    )

    def body(*args):
        heads, width = args[11].shape
        features = args[12].shape[1]
        block, model_width = args[0].shape[1:]
        fits = (
            lax.axis_size("tp") == 2
            and lax.axis_size("fs") == 4
            and lax.axis_size("sp") == 4
            and heads == 4
            and width == 128
            and features == 8 * width
            and model_width == 2 * features
            and block == 2 * width
        )
        return (by_group if fits else per_device)(*args)

    return jax.shard_map(
        body,
        mesh=mesh,
        in_specs=placed,
        out_specs=P("fs", ("sp", "tp"), None),
        check_vma=False,
    )
```

time: 149 us -> 107 us (0.72)
  Pallas kernels: 135 us -> 105 us
  local copies, waits for them, and re-layouts: 10.1 us -> 1.88 us
  other arithmetic: 3.79 us -> 0 us
    pallas_call x4 -> x1, Pallas kernels: 135 us -> 105 us  [by_group(): pl.pallas_call(functools.partial(layer_kernel, n_sp), out_shape=jax.Shape...]
    dynamic_slice x5 -> x0, local copies, waits for them, and re-layouts: 4.96 us -> none  [the longest x1 1.26 us: by_head(): gain = lax.dynamic_slice_in_dim(head_gain, sp, 1, 0)]
    convert_element_type x10 -> x0, other arithmetic: 3.78 us -> none  [the longest x1 2.54 us: pool_window(): return (window_sum / counted - centre).astype(jnp.bfloat16)]
    unnamed x12 -> x1, local copies, waits for them, and re-layouts: 3.07 us -> 1.88 us
where the time goes in v1:
time: 107 us
  Pallas kernels  105 us (98%)
  local copies, waits for them, and re-layouts  1.88 us (2%)
    pallas_call x1, Pallas kernels, by_group(): pl.pallas_call(functools.partial(layer_kernel, n_sp), out_shape=jax.Shape...  105 us

profile of v1, /device:TPU:0, one launch (start us, length us, event | category | flops | bytes accessed | tf_op | source)
XLA Modules:
  0.0 106.7 jit_solution(6990169611587745285)
XLA Ops:
  0.0 104.8 %layer.1 = bf16[128,2048]{1,0:T(8,128)(2,1)} custom-call(bf16[256,2048]{1,0:T(8,128)(2,1)} %bitcast.7, f32[1,2048]{1,0:T(1,128)} %bitcast.9, bf16[128,512]{1,0:T(8,128)(2,1)} %qw.1, bf16[128,512]{1,0:T(8,128)(2,1)} %kw.1, bf16[128,512]{1,0:T(8,128)(2,1)} %vw.1, bf16[128,512]{1,0:T(8,128)(2,1)} %ow.1, bf16[4,4,2048]{2,1,0:T(4,128)(2,1)} %gate_ref.1, ...), custom_call_target="tpu_custom_call" | custom-call | tf_op jit(solution)/shard_map/layer/pallas_call | solution.py:879
  104.8 1.9 %copy.17 = bf16[1,128,2048]{2,1,0:T(8,128)(2,1)} copy(bf16[1,128,2048]{2,1,0:T(8,128)(2,1)} %bitcast.6) | data formatting | bytes 1048576

commit v2 on v1

--- a/solution.py
+++ b/solution.py
@@ -361,10 +361,10 @@
     hgain_ref, pw, mw, fw,
     o_ref,
     x_all, normed, w_all, stage, transit, gmat, dec, init, nrm, proj_a, proj_b, pool_buf, act,
-    flat, cols, level_rows, msg_out, msg_in, state_out, state_in, halo_out, halo_in,
+    within, dens, values_t, pre_rows, flat, cols, run_rows, aux_out, aux_in, state_out, state_in, halo_tok,
     give, take, total, s1, l1, s2, l2,
     loc_w, loc_s, x_ss, x_rs, p_ss, p_rs, h_ss, h_rs, y_ss, y_rs,
-    tz_ss, tz_rs, tx_ss, tx_rs, tw_ss, tw_rs, d_ss, d_rs, i_ss, i_rs, m_ss, m_rs,
+    token_p_ss, token_p_rs, tx_ss, tx_rs, tw_ss, tw_rs, d_ss, d_rs, i_ss, i_rs, m_ss, m_rs, e_ss, e_rs,
     sw_ss, sw_rs, r1_ss, r1_rs, r2_ss, r2_rs,
 ):
     block, width = token_ref.shape
@@ -373,7 +373,7 @@
     feat = pw.shape[1] // 4
     half = block // 2
     span = 2 * block
-    pieces_t = 2
+    pieces_t = token_p_ss.shape[0]
     part = half // pieces_t
     z, fs, c = lax.axis_index("sp"), lax.axis_index("fs"), lax.axis_index("tp")
     y, x = fs // 2, lax.rem(fs, 2)
@@ -396,9 +396,15 @@
     def at(start, size):
         return pl.ds(pl.multiple_of(start, size), size)
 
+    inner = p != h
+    to_m = {"sp": n_sp - 1 - z}
     barrier = pltpu.get_barrier_semaphore()
     for device in (to_x, to_y, to_p, to_h, to_c):
         pl.semaphore_signal(barrier, inc=1, device_id=device, device_id_type=MESH)
+
+    @pl.when(inner)
+    def _():
+        pl.semaphore_signal(barrier, inc=1, device_id=to_m, device_id_type=MESH)
 
     groups = (((qw, hw), (kw, hw), (vw, hw)), ((ow, hw), (pw, feat)), ((mw, hw), (fw, feat)))
     quarters = (quarter, 2 * p + 1 - x, 2 * (1 - p) + 1 - x, 2 * (1 - p) + x)
@@ -456,11 +462,9 @@
         ref = w_all.at[g, row_block(source, y, 1 - x if s else x)]
         return remote(ref, ref, h_ss.at[g, k, s], h_rs.at[g, k, s], to_h)
 
-    def y_copy(g, k, s, incoming=False):
-        ref = w_all.at[
-            g, row_block((z, zn, zf, zfn)[k], 1 - y if incoming else y, 1 - x if s else x)
-        ]
-        return remote(ref, ref, y_ss.at[g, k, s], y_rs.at[g, k, s], to_y)
+    def y_copy(g, plane, s, incoming=False):
+        ref = w_all.at[g, row_block(plane, 1 - y if incoming else y, 1 - x if s else x)]
+        return remote(ref, ref, y_ss.at[g, plane, s], y_rs.at[g, plane, s], to_y)
 
     sent = []
 
@@ -468,38 +472,61 @@
         copy.start()
         sent.append(copy)
 
-    def begin(g):
-        for copy in locals_[g]:
-            copy.wait()
+    def ready(g, slots):
+        size = len(groups[g])
+        for place, slot in enumerate((1, 2, 3, 0)):
+            if slot in slots:
+                for copy in locals_[g][place * size : (place + 1) * size]:
+                    copy.wait()
+
+    def begin_x(g):
+        ready(g, (1, 2))
         go(x_copy(g, 1))
         go(x_copy(g, 0))
+
+    def begin_p(g):
+        ready(g, (3,))
         go(p_copy(g, 0))
+
+    def begin_h(g):
         go(h_copy(g, 0, 0))
-        go(y_copy(g, 0, 0))
+
+    def begin_z(g):
+        begin_p(g)
+        if g == 0:
+            ready(g, (0,))
+        begin_h(g)
+
+    def begin_y(g):
+        if g:
+            ready(g, (0,))
+        go(y_copy(g, z, 0))
 
     def after_x(g):
         x_copy(g, 1, True).wait_recv()
         go(p_copy(g, 1))
         x_copy(g, 0, True).wait_recv()
         go(h_copy(g, 0, 1))
-        go(y_copy(g, 0, 1))
+        go(y_copy(g, z, 1))
 
     def after_p(g):
         for s in range(2):
             p_copy(g, s, True).wait_recv()
             go(h_copy(g, 1, s))
-            go(y_copy(g, 1, s))
-
-    def after_h(g):
-        for k in range(2):
-            for s in range(2):
-                h_copy(g, k, s, True).wait_recv()
-                go(y_copy(g, 2 + k, s))
-
-    def after_y(g):
-        for k in range(4):
-            for s in range(2):
-                y_copy(g, k, s, True).wait_recv()
+            go(y_copy(g, zn, s))
+
+    def after_h(g, k):
+        for s in range(2):
+            h_copy(g, k, s, True).wait_recv()
+            go(y_copy(g, (zf, zfn)[k], s))
+
+    def after_y(g, plane):
+        for s in range(2):
+            y_copy(g, plane, s, True).wait_recv()
+
+    def all_y(g):
+        for plane in (z, zn, zf, zfn):
+            after_y(g, plane)
 
     def token_rows(j, b, side, i):
         return at((2 * j + b) * block + side * half + i * part, part)
@@ -508,7 +535,7 @@
         b = 1 - p if incoming else p
         dst = x_all.at[token_rows(x, b, c, i)]
         src = dst if incoming else token_ref.at[at(c * half + i * part, part)]
-        return remote(src, dst, tz_ss.at[i], tz_rs.at[i], to_p)
+        return remote(src, dst, token_p_ss.at[i], token_p_rs.at[i], to_p)
 
     def token_x(kind, i, incoming=False):
         b = 1 - p if kind else p
@@ -522,6 +549,32 @@
         j, b = places[which]
         ref = x_all.at[token_rows(j, b, other if incoming else c, i)]
         return remote(ref, ref, tw_ss.at[which, i], tw_rs.at[which, i], to_c)
+
+    edge_rows = halo_tok.shape[1]
+
+    def edge_copy(which):
+        return remote(
+            token_ref.at[at((1 - h) * (block - edge_rows), edge_rows)], halo_tok.at[x],
+            e_ss.at[which], e_rs.at[0], (to_h, to_m)[which],
+        )
+
+    def edges(action):
+        @pl.when(inner)
+        def _():
+            for which in range(2):
+                action(edge_copy(which))
+
+    def edge_x(incoming=False):
+        ref = halo_tok.at[1 - x if incoming else x]
+        return remote(ref, ref, e_ss.at[2], e_rs.at[1], to_x)
+
+    def normalise_edges():
+        wide = halo_tok[...].reshape(2 * edge_rows, width).astype(jnp.float32)
+        normed[4 * block :, :] = (
+            wide
+            * lax.rsqrt(jnp.mean(wide * wide, axis=-1, keepdims=True) + norm_eps)
+            * gain_ref[...]
+        ).astype(jnp.bfloat16)
 
     def decay_p(incoming=False):
         dst = dec.at[x, 1 - p if incoming else p]
@@ -551,261 +604,312 @@
             return carry
 
         lax.fori_loop(0, block // step, body, 0)
-
-    pl.semaphore_wait(barrier, 5)
-    begin(0)
-    for i in range(pieces_t):
-        go(token_p(i))
-        go(token_x(0, i))
+        here = at((2 * j + b) * block, block)
+        pre_rows[2 * j + b] = transposed_dot(normed[here, :], gmat[...]).T[:8]
+
+    def scoped(name, function, *args):
+        with jax.named_scope(name):
+            return function(*args)
+
+    def token_arrivals_p(these):
+        for i in these:
+            token_p(i, True).wait_recv()
+            go(token_swap(0, i))
+            go(token_x(1, i))
+
+    def token_arrivals_x(kind, these):
+        for i in these:
+            token_x(kind, i, True).wait_recv()
+            go(token_swap(1 + kind, i))
+
+    def swapped(which):
+        for i in range(pieces_t):
+            token_swap(which, i, True).wait_recv()
+        normalise(*places[which])
+
+    def pick_gates():
+        gmat[...] = jnp.zeros_like(gmat)
+        pick = lax.broadcasted_iota(jnp.int32, (4, width), 0) == quarter
+        row16 = lax.broadcasted_iota(jnp.int32, (16, width), 0)
+        gates16 = jnp.zeros((16, width), jnp.float32)
+        for i in range(4):
+            row = jnp.sum(
+                jnp.where(pick, gate_ref[i].astype(jnp.float32), 0.0), axis=0, keepdims=True
+            )
+            gates16 = jnp.where((row16 == i) | (row16 == i + 4), row, gates16)
+        gmat[0:16, :] = gates16.astype(jnp.bfloat16)
+
+    scoped("barrier", pl.semaphore_wait, barrier, 5 + inner.astype(jnp.int32))
+    begin_x(0)
+    begin_z(0)
+    begin_y(0)
+    edges(lambda copy: copy.start())
     own_decay.wait()
     go(decay_p())
     go(decay_x(0))
-    gmat[...] = jnp.zeros_like(gmat)
-    pick = lax.broadcasted_iota(jnp.int32, (4, width), 0) == quarter
-    row16 = lax.broadcasted_iota(jnp.int32, (16, width), 0)
-    gates16 = jnp.zeros((16, width), jnp.float32)
-    for i in range(4):
-        row = jnp.sum(
-            jnp.where(pick, gate_ref[i].astype(jnp.float32), 0.0), axis=0, keepdims=True
-        )
-        gates16 = jnp.where((row16 == i) | (row16 == i + 4), row, gates16)
-    gmat[0:16, :] = gates16.astype(jnp.bfloat16)
-    own_tokens.wait()
-    normalise(x, p)
-    after_x(0)
-    begin(1)
+    go(token_p(0))
+    begin_x(1)
+    for i in range(pieces_t):
+        go(token_x(0, i))
+    begin_y(1)
+    scoped("pick", pick_gates)
+    scoped("tok_own", own_tokens.wait)
+    scoped("norm_own", normalise, x, p)
+    scoped("after_x_0", after_x, 0)
+    remote(halo_tok.at[x], halo_tok.at[x], e_ss.at[0], e_rs.at[0], to_h).wait_recv()
+    go(edge_x())
+    scoped("after_p_0", after_p, 0)
+    for i in range(1, pieces_t):
+        go(token_p(i))
+    begin_z(1)
+    scoped("after_x_1", after_x, 1)
+    scoped("after_h_0", after_h, 0, 0)
+    scoped("tok_p", token_arrivals_p, (0,))
+    scoped("tok_x0", token_arrivals_x, 0, (0, 1))
+    scoped("after_h_0", after_h, 0, 1)
+    scoped("tok_p", token_arrivals_p, (1,))
+    scoped("tok_x0", token_arrivals_x, 0, (2, 3))
+    scoped("norm_x", swapped, 1)
+    edge_x(True).wait_recv()
+    normalise_edges()
+    scoped("tok_p", token_arrivals_p, (2, 3))
+    decay_p(True).wait_recv()
+    go(decay_x(1))
     go(init_x(0))
     go(init_x(1))
-    for i in range(pieces_t):
-        token_p(i, True).wait_recv()
-        go(token_swap(0, i))
-        go(token_x(1, i))
-    decay_p(True).wait_recv()
-    go(decay_x(1))
-    after_p(0)
-    for i in range(pieces_t):
-        token_x(0, i, True).wait_recv()
-        go(token_swap(1, i))
-    for i in range(pieces_t):
-        token_swap(0, i, True).wait_recv()
-    normalise(x, 1 - p)
-    after_x(1)
-    begin(2)
-    for i in range(pieces_t):
-        token_swap(1, i, True).wait_recv()
-    normalise(1 - x, p)
-    after_h(0)
-    for i in range(pieces_t):
-        token_x(1, i, True).wait_recv()
-        go(token_swap(2, i))
-    after_p(1)
-    for i in range(pieces_t):
-        token_swap(2, i, True).wait_recv()
-    normalise(1 - x, 1 - p)
+    begin_x(2)
+    begin_y(2)
+    scoped("norm_p", swapped, 0)
+    scoped("after_y_0", all_y, 0)
+
+    def project(g, place, store):
+        i = 2 * place[0] + place[1]
+        store(i, jnp.dot(
+            normed[at(i * block, block), :], w_all[g], preferred_element_type=jnp.float32
+        ).astype(jnp.bfloat16))
+
+    def store_a(i, value):
+        proj_a[at(i * block, block), :] = value
+
+    for place in ((x, p), places[0], places[1]):
+        scoped("project_0", project, 0, place, store_a)
+    scoped("tok_x1", token_arrivals_x, 1, (0, 1))
+    scoped("after_p_1", after_p, 1)
+    scoped("tok_x1", token_arrivals_x, 1, (2, 3))
+    scoped("after_h_1", after_h, 1, 0)
+    scoped("norm_px", swapped, 2)
     decay_x(0, True).wait_recv()
     decay_x(1, True).wait_recv()
 
-    tall = []
-    for j in range(2):
-        pieces = []
-        for b in range(2):
-            pre = transposed_dot(normed[(2 * j + b) * block : (2 * j + b + 1) * block, :], gmat[...])
-            pieces.append(pre.T[:8])
-        tall.append(jnp.concatenate(pieces, axis=1))
-    row8 = lax.broadcasted_iota(jnp.int32, (8, span), 0)
-    gates = jnp.where(row8 < 4, tall[0], tall[1])
-    extra = jnp.zeros((8, span), jnp.float32)
-    for i in range(4):
-        gates = gates + jnp.where((row8 == i) | (row8 == i + 4), bias_ref[i, quarter], 0.0)
-    for j in range(2):
-        for direction in range(2):
-            value = jnp.concatenate(
-                [dec[j, b, direction, pl.ds(quarter, 1), :] for b in range(2)], axis=1
+    with jax.named_scope("gates"):
+        tall = []
+        for j in range(2):
+            tall.append(jnp.concatenate([pre_rows[2 * j], pre_rows[2 * j + 1]], axis=1))
+        row8 = lax.broadcasted_iota(jnp.int32, (8, span), 0)
+        gates = jnp.where(row8 < 4, tall[0], tall[1])
+        extra = jnp.zeros((8, span), jnp.float32)
+        for i in range(4):
+            gates = gates + jnp.where((row8 == i) | (row8 == i + 4), bias_ref[i, quarter], 0.0)
+        for j in range(2):
+            for direction in range(2):
+                value = jnp.concatenate(
+                    [dec[j, b, direction, pl.ds(quarter, 1), :] for b in range(2)], axis=1
+                )
+                extra = jnp.where(row8 == 4 * j + 1 + 2 * direction, value, extra)
+        forget = jnp.minimum(gates, 0.0) - jnp.log1p(jnp.exp(-jnp.abs(gates))) + extra
+        sum_f = pltpu.roll(scan_lanes(forget, jnp.add, 0.0, False), 7, 0)
+        sum_b = pltpu.roll(scan_lanes(forget, jnp.add, 0.0, True), 7, 0)
+        level_f = gates - sum_f
+        level_b = gates - sum_b
+        run_f = scan_lanes(level_f, jnp.maximum, -1e30, False)
+        run_b = scan_lanes(level_b, jnp.maximum, -1e30, True)
+        top_f = jnp.maximum(run_f[:, span - 1 : span], 0.0)
+        top_b = jnp.maximum(run_b[:, 0:1], 0.0)
+        end_f = sum_f[:, span - 1 : span] + top_f
+        end_b = sum_b[:, 0:1] + top_b
+        aux_out[2] = jnp.broadcast_to(jnp.where(low, end_f, end_b), (8, hw))
+
+    def message(which, incoming=False):
+        src = (aux_out, state_out)[which]
+        dst = (aux_in, state_in)[which]
+        return remote(dst if incoming else src, dst, m_ss.at[which], m_rs.at[which], to_h)
+
+    scoped("project_0", project, 0, places[2], store_a)
+
+    with jax.named_scope("state"):
+        scale_bits = -0.5 * math.log2(hw)
+        lf2 = level_f * LOG2E + scale_bits
+        lb2 = level_b * LOG2E + scale_bits
+        own_init.wait()
+        own_nrm.wait()
+        init_x(0, True).wait_recv()
+        init_x(1, True).wait_recv()
+        leave_f = jnp.exp2(lf2 - top_f * LOG2E)
+        leave_b = jnp.exp2(lb2 - top_b * LOG2E)
+        keep_f = jnp.exp(-top_f)
+        keep_b = jnp.exp(-top_b)
+        for j in range(2):
+            here = slice(j * span, (j + 1) * span)
+            own = jnp.where(low, leave_f[4 * j : 4 * j + 1], leave_b[4 * j + 2 : 4 * j + 3])
+            kept = jnp.where(low, keep_f[4 * j : 4 * j + 1], keep_b[4 * j + 2 : 4 * j + 3])
+            values = proj_a[here, 2 * hw : 3 * hw].astype(jnp.float32).T
+            values_t[j] = values.astype(jnp.bfloat16)
+            values = values * own
+            lhs = jnp.concatenate(
+                [values, jnp.broadcast_to(own, (8, span))], axis=0
+            ).astype(jnp.bfloat16)
+            grown = jnp.dot(lhs, proj_a[here, hw : 2 * hw], preferred_element_type=jnp.float32)
+            state_out[j] = (kept * init[j] + grown[:hw]).astype(jnp.bfloat16)
+            aux_out[j] = kept * nrm[j, h, pl.ds(quarter, 1), :] + grown[hw:]
+    go(message(0))
+    go(message(1))
+    begin_p(2)
+    begin_h(2)
+
+    with jax.named_scope("levels"):
+        flat[16:, :] = jnp.zeros_like(flat[16:, :])
+        flat[0:8, :] = lf2
+        flat[8:16, :] = lb2
+        cols[...] = flat[...].T
+        run_rows[0] = run_f * LOG2E
+        run_rows[1] = run_b * LOG2E
+
+    def attend(j):
+        here = slice(j * span, (j + 1) * span)
+        f, b = 4 * j, 4 * j + 2
+        levels = [jnp.broadcast_to(cols[:, k : k + 1], (span, half)) for k in (f, 8 + b)]
+        for i in range(4):
+            r0 = i * half
+            mine = slice(j * span + r0, j * span + r0 + half)
+            score = transposed_dot(proj_a[here, hw : 2 * hw], proj_a[mine, 0:hw])
+            for which, first, last in ((0, 0, r0 + half), (1, r0, span)):
+                row = (f, b)[which]
+                peak = run_rows[which, row : row + 1, r0 : r0 + half]
+                weight = jnp.exp2(levels[which][first:last] - peak) * score[first:last]
+                s = first + lax.broadcasted_iota(jnp.int32, weight.shape, 0)
+                t = r0 + lax.broadcasted_iota(jnp.int32, weight.shape, 1)
+                weight = jnp.where(s >= t if which else s <= t, weight, 0.0)
+                within[which, j, :, r0 : r0 + half] = jnp.dot(
+                    values_t[j, :, first:last], weight.astype(jnp.bfloat16),
+                    preferred_element_type=jnp.float32,
+                )
+                dens[which, j : j + 1, r0 : r0 + half] = jnp.sum(weight, axis=0, keepdims=True)
+
+    scoped("attend_0", attend, 0)
+    scoped("attend_1", attend, 1)
+    scoped("after_x_2", after_x, 2)
+    scoped("after_h_1", after_h, 1, 1)
+    scoped("after_p_2", after_p, 2)
+    scoped("after_y_1", all_y, 1)
+
+    def project_b():
+        for i in range(4):
+            last_rows = 2 * edge_rows if i == 3 else 0
+            value = jnp.dot(
+                normed[i * block : (i + 1) * block + last_rows, :], w_all[1],
+                preferred_element_type=jnp.float32,
+            ).astype(jnp.bfloat16)
+            proj_b[i * block : (i + 1) * block, :] = value[:block, :hw]
+            start = 8 + (i % 2) * block
+            pool_buf[i // 2, start : start + block, :] = value[:block, hw:].astype(jnp.float32)
+        beyond = value[block:, hw:].astype(jnp.float32)
+        zero = jnp.zeros((8, feat), jnp.float32)
+        for j in range(2):
+            mine = beyond[j * edge_rows : (j + 1) * edge_rows]
+            pool_buf[j, 0:8, :] = jnp.where(low, zero, mine[edge_rows - 8 :])
+            pool_buf[j, span + 8 : span + 16, :] = jnp.where(low, mine[:8], zero)
+
+    scoped("project_1", project_b)
+    scoped("state_in", message(1, True).wait_recv)
+    scoped("aux_in", message(0, True).wait_recv)
+
+    with jax.named_scope("enter"):
+        arrived = aux_in[2, :, 0:1]
+        enter_f = jnp.where(low, 0.0, arrived)
+        enter_b = jnp.where(low, arrived, 0.0)
+        factors = []
+        for run, enter, summed in ((run_f, enter_f, sum_f), (run_b, enter_b, sum_b)):
+            peak = jnp.maximum(run, enter)
+            factors.append(
+                (jnp.exp(run - peak), jnp.exp(enter - peak), jnp.exp(-(summed + peak)))
             )
-            extra = jnp.where(row8 == 4 * j + 1 + 2 * direction, value, extra)
-    forget = jnp.minimum(gates, 0.0) - jnp.log1p(jnp.exp(-jnp.abs(gates))) + extra
-    sum_f = pltpu.roll(scan_lanes(forget, jnp.add, 0.0, False), 7, 0)
-    sum_b = pltpu.roll(scan_lanes(forget, jnp.add, 0.0, True), 7, 0)
-    level_f = gates - sum_f
-    level_b = gates - sum_b
-    run_f = scan_lanes(level_f, jnp.maximum, -1e30, False)
-    run_b = scan_lanes(level_b, jnp.maximum, -1e30, True)
-    top_f = jnp.maximum(run_f[:, span - 1 : span], 0.0)
-    top_b = jnp.maximum(run_b[:, 0:1], 0.0)
-    end_f = sum_f[:, span - 1 : span] + top_f
-    end_b = sum_b[:, 0:1] + top_b
-    msg_out[...] = jnp.broadcast_to(jnp.where(low, end_f, end_b), msg_out.shape)
-
-    def message(which, incoming=False):
-        src = (msg_out, state_out, halo_out)[which]
-        dst = (msg_in, state_in, halo_in)[which]
-        return remote(dst if incoming else src, dst, m_ss.at[which], m_rs.at[which], to_h)
-
-    go(message(0))
-
-    after_y(0)
-
-    def project(g, store):
-        def body(i, carry):
-            here = at(i * block, block)
-            store(i, jnp.dot(
-                normed[here, :], w_all[g], preferred_element_type=jnp.float32
-            ).astype(jnp.bfloat16))
-            return carry
-
-        lax.fori_loop(0, 4, body, 0)
-
-    def store_a(i, value):
-        proj_a[at(i * block, block), :] = value
-
-    project(0, store_a)
-    after_h(1)
-
-    message(0, True).wait_recv()
-    arrived = msg_in[:, 0:1]
-    enter_f = jnp.where(low, 0.0, arrived)
-    enter_b = jnp.where(low, arrived, 0.0)
-    scale_bits = -0.5 * math.log2(hw)
-    lf2 = level_f * LOG2E + scale_bits
-    lb2 = level_b * LOG2E + scale_bits
-    peak_f = jnp.maximum(run_f, enter_f)
-    peak_b = jnp.maximum(run_b, enter_b)
-    level_rows[0:8, :] = lf2
-    level_rows[8:16, :] = lb2
-    flat[48:, :] = jnp.zeros_like(flat[48:, :])
-    flat[0:8, :] = peak_f * LOG2E
-    flat[8:16, :] = peak_b * LOG2E
-    flat[16:24, :] = jnp.exp(enter_f - peak_f)
-    flat[24:32, :] = jnp.exp(enter_b - peak_b)
-    flat[32:40, :] = jnp.exp(-(sum_f + peak_f))
-    flat[40:48, :] = jnp.exp(-(sum_b + peak_b))
-    cols[...] = flat[...].T
-
-    own_init.wait()
-    own_nrm.wait()
-    init_x(0, True).wait_recv()
-    init_x(1, True).wait_recv()
-    leave_f = jnp.exp2(lf2 - top_f * LOG2E)
-    leave_b = jnp.exp2(lb2 - top_b * LOG2E)
-    keep_f = jnp.exp(-top_f)
-    keep_b = jnp.exp(-top_b)
-    starts = []
-    for j in range(2):
-        here = slice(j * span, (j + 1) * span)
-        own = jnp.where(low, leave_f[4 * j : 4 * j + 1], leave_b[4 * j + 2 : 4 * j + 3])
-        kept = jnp.where(low, keep_f[4 * j : 4 * j + 1], keep_b[4 * j + 2 : 4 * j + 3])
-        values = proj_a[here, 2 * hw : 3 * hw].astype(jnp.float32).T * own
-        lhs = jnp.concatenate(
-            [values, jnp.broadcast_to(own, (8, span))], axis=0
-        ).astype(jnp.bfloat16)
-        grown = jnp.dot(lhs, proj_a[here, hw : 2 * hw], preferred_element_type=jnp.float32)
-        start = jnp.concatenate(
-            [init[j], jnp.broadcast_to(nrm[j, h, pl.ds(quarter, 1), :], (8, hw))], axis=0
-        )
-        starts.append(start)
-        state_out[j] = kept * start + grown
-    go(message(1))
-
-    after_y(1)
-
-    def store_b(i, value):
-        proj_b[at(i * block, block), :] = value[:, :hw]
-        pool_buf[i // 2, pl.ds(pl.multiple_of(8 + lax.rem(i, 2) * block, 8), block), :] = value[
-            :, hw:
-        ].astype(jnp.float32)
-
-    project(1, store_b)
-    for j in range(2):
-        halo_out[j] = jnp.where(low, pool_buf[j, span : span + 8, :], pool_buf[j, 8:16, :])
-    go(message(2))
-    after_x(2)
-    after_p(2)
-
-    message(1, True).wait_recv()
-    for j in range(2):
-        here = slice(j * span, (j + 1) * span)
-        front_start = jnp.where(low, starts[j], state_in[j])
-        rear_start = jnp.where(low, state_in[j], starts[j])
+
+    def finish(j):
+        own_n = jnp.broadcast_to(nrm[j, h, pl.ds(quarter, 1), :], (8, hw))
+        there = state_in[j].astype(jnp.float32)
         carry_in = jnp.concatenate(
-            [front_start[:hw], rear_start[:hw], front_start[hw:], rear_start[hw:]], axis=0
-        )
-        carry_in = jnp.concatenate(
-            [carry_in, jnp.zeros((3 * hw - carry_in.shape[0], hw), jnp.float32)], axis=0
+            [
+                jnp.where(low, init[j], there),
+                jnp.where(low, there, init[j]),
+                jnp.where(low, own_n, aux_in[j]),
+                jnp.where(low, aux_in[j], own_n),
+            ],
+            axis=0,
         )
         coarse = carry_in.astype(jnp.bfloat16)
         fine = (carry_in - coarse.astype(jnp.float32)).astype(jnp.bfloat16)
+        q = proj_a[j * span : (j + 1) * span, 0:hw]
+        carry = transposed_dot(
+            jnp.concatenate([coarse, fine], axis=1), jnp.concatenate([q, q], axis=1)
+        )
+        both = []
+        for which in range(2):
+            row = 4 * j + 2 * which
+            grow, decay, floor = (part[row : row + 1] for part in factors[which])
+            den0 = carry[2 * hw + 8 * which : 2 * hw + 8 * which + 1]
+            den = grow * dens[which, j : j + 1, :] + decay * den0
+            share = 1.0 / jnp.maximum(jnp.abs(den), floor)
+            both.append(
+                (grow * share) * within[which, j]
+                + (decay * share) * carry[which * hw : (which + 1) * hw]
+            )
+        summed = both[0] + both[1]
+        summed = summed * lax.rsqrt(jnp.mean(summed * summed, axis=0, keepdims=True) + norm_eps)
+        out = (
+            summed.T
+            * hgain_ref[pl.ds(quarter, 1), :]
+            * jax.nn.sigmoid(proj_b[j * span : (j + 1) * span, :].astype(jnp.float32))
+        ).astype(jnp.bfloat16)
         for i in range(4):
-            r0 = i * half
-            mine = slice(j * span + r0, j * span + r0 + half)
-            q = proj_a[mine, 0:hw]
-            carry = transposed_dot(q, coarse) + transposed_dot(q, fine)
-            score = transposed_dot(q, proj_a[here, hw : 2 * hw])
-            col = cols[r0 : r0 + half, :]
-
-            def direction(first, last, level, peak, decay, floor, got, den0, rear):
-                weight = jnp.exp2(level[:, first:last] - peak) * score[:, first:last]
-                t = r0 + lax.broadcasted_iota(jnp.int32, weight.shape, 0)
-                s = first + lax.broadcasted_iota(jnp.int32, weight.shape, 1)
-                weight = jnp.where(s >= t if rear else s <= t, weight, 0.0)
-                num = decay * got + jnp.dot(
-                    weight.astype(jnp.bfloat16),
-                    proj_a[j * span + first : j * span + last, 2 * hw : 3 * hw],
-                    preferred_element_type=jnp.float32,
-                )
-                den = decay * den0 + jnp.sum(weight, axis=1, keepdims=True)
-                return num / jnp.maximum(jnp.abs(den), floor)
-
-            f, b = 4 * j, 4 * j + 2
-            summed = direction(
-                0, r0 + half, level_rows[f : f + 1, :], col[:, f : f + 1],
-                col[:, 16 + f : 17 + f], col[:, 32 + f : 33 + f],
-                carry[:, :hw], carry[:, 2 * hw : 2 * hw + 1], False,
-            ) + direction(
-                r0, span, level_rows[8 + b : 9 + b, :], col[:, 8 + b : 9 + b],
-                col[:, 24 + b : 25 + b], col[:, 40 + b : 41 + b],
-                carry[:, hw : 2 * hw], carry[:, 2 * hw + 8 : 2 * hw + 9], True,
-            )
-            out = (
-                summed
-                * lax.rsqrt(jnp.mean(summed * summed, axis=-1, keepdims=True) + norm_eps)
-                * hgain_ref[pl.ds(quarter, 1), :]
-                * jax.nn.sigmoid(proj_b[mine, :].astype(jnp.float32))
-            )
             place = (i % 2) * span + (2 * j + i // 2) * half
-            act[place : place + half, 0:hw] = out.astype(jnp.bfloat16)
-        if j == 0:
-            after_h(2)
-
-    message(2, True).wait_recv()
-    for j in range(2):
-        zero = jnp.zeros((8, feat), jnp.float32)
-        pool_buf[j, 0:8, :] = jnp.where(low, zero, halo_in[j])
-        pool_buf[j, span + 8 : span + 16, :] = jnp.where(low, halo_in[j], zero)
-    group = (c * 4 + quarter) * feat * 4 // width
-    for k in range(4):
-
-        @pl.when(group == k)
-        def _(k=k):
-            reach = 2 ** k
-            t = h * span + lax.broadcasted_iota(jnp.int32, (span, 1), 0)
-            counted = jnp.minimum(t + reach - 1, n_sp * block - 1) - jnp.maximum(t - reach, 0) + 1
-            counted = counted.astype(jnp.float32)
-            length = span + 16
-            for j in range(2):
-                window = pool_buf[j]
-                for e in range(k + 1):
-                    window = window + pltpu.roll(window, length - 2 ** e, 0)
-                if reach < 8:
-                    window = pltpu.roll(window, length - (8 - reach), 0)
-                value = window[:span] / counted - pool_buf[j, 8 : 8 + span, :]
-                value = value.astype(jnp.bfloat16)
-                for i in range(4):
-                    place = (i % 2) * span + (2 * j + i // 2) * half
-                    act[place : place + half, hw:] = value[i * half : (i + 1) * half]
-
-    after_y(2)
+            act[place : place + half, 0:hw] = out[i * half : (i + 1) * half]
+
+    scoped("finish", finish, 0)
+    scoped("finish", finish, 1)
+
+    with jax.named_scope("pooling"):
+        group = (c * 4 + quarter) * feat * 4 // width
+        for k in range(4):
+
+            @pl.when(group == k)
+            def _(k=k):
+                reach = 2 ** k
+                t = h * span + lax.broadcasted_iota(jnp.int32, (span, 1), 0)
+                counted = jnp.minimum(t + reach - 1, n_sp * block - 1) - jnp.maximum(t - reach, 0) + 1
+                counted = counted.astype(jnp.float32)
+                length = span + 16
+                for j in range(2):
+                    window = pool_buf[j]
+                    for e in range(k + 1):
+                        window = window + pltpu.roll(window, length - 2 ** e, 0)
+                    if reach < 8:
+                        window = pltpu.roll(window, length - (8 - reach), 0)
+                    value = window[:span] / counted - pool_buf[j, 8 : 8 + span, :]
+                    value = value.astype(jnp.bfloat16)
+                    for i in range(4):
+                        place = (i % 2) * span + (2 * j + i // 2) * half
+                        act[place : place + half, hw:] = value[i * half : (i + 1) * half]
+
     count = give.shape[0]
     tile = width // count
+    each = count // 4
+    planes = (2 * h, 2 * h + 1, 2 * (1 - h), 2 * (1 - h) + 1)
+
+    def columns_of(n):
+        return at(planes[n // each] * (width // 4) + (n % each) * tile, tile)
+
+    def mixed(n):
+        return n % 2 == 1
 
     def swap(n):
         return remote(give.at[n], take.at[n], sw_ss.at[n], sw_rs.at[n], to_c)
@@ -814,47 +918,78 @@
         dst = l1.at[n, slot]
         return remote(
             dst if incoming else s1.at[n, slot], dst, r1_ss.at[n, slot], r1_rs.at[n, slot],
-            to_p if n % 2 else to_x,
+            to_p if mixed(n) else to_x,
         )
 
     def second_stage(n, incoming=False):
         return remote(
             l2.at[n] if incoming else s2.at[n], l2.at[n], r2_ss.at[n], r2_rs.at[n],
-            to_x if n % 2 else to_p,
+            to_x if mixed(n) else to_p,
         )
 
     def product(side, n):
-        return transposed_dot(act[at(side * span, span), :], w_all[2, n * tile : (n + 1) * tile, :])
-
-    for n in range(count):
-        give[n] = product(other, n).astype(jnp.bfloat16).reshape(give.shape[1:])
-        go(swap(n))
+        return transposed_dot(act[at(side * span, span), :], w_all[2, columns_of(n), :])
+
     home = 2 * x + p
     both = 2 * (1 - x) + 1 - p
-    for n in range(count):
+
+    def first(n):
         part_sum = product(c, n)
         swap(n).wait_recv()
         total[n] = part_sum.reshape(total.shape[1:]) + take[n].astype(jnp.float32)
         near, middle = 2 * (1 - x) + p, 2 * x + 1 - p
-        if n % 2:
+        if mixed(n):
             near, middle = middle, near
         s1[n, 1] = total[n, both].astype(jnp.bfloat16)
         go(first_stage(n, 1))
         s1[n, 0] = total[n, near].astype(jnp.bfloat16)
         go(first_stage(n, 0))
-    for n in range(count):
-        middle = 2 * (1 - x) + p if n % 2 else 2 * x + 1 - p
+
+    def second(n):
+        middle = 2 * (1 - x) + p if mixed(n) else 2 * x + 1 - p
         first_stage(n, 1, True).wait_recv()
         s2[n] = (total[n, middle] + l1[n, 1].astype(jnp.float32)).astype(jnp.bfloat16)
         go(second_stage(n))
-    for n in range(count):
+
+    def last(n):
         first_stage(n, 0, True).wait_recv()
         second_stage(n, True).wait_recv()
-        o_ref[:, n * tile : (n + 1) * tile] = (
+        o_ref[:, columns_of(n)] = (
             total[n, home] + l1[n, 0].astype(jnp.float32) + l2[n].astype(jnp.float32)
         ).astype(jnp.bfloat16)
-    for copy in sent:
-        copy.wait_send()
+
+    for q in range(4):
+        mine = range(q * each, (q + 1) * each)
+        scoped("plane#q=%d" % q, after_y, 2, planes[q])
+        with jax.named_scope("give#q=%d" % q):
+            for n in mine:
+                give[n] = product(other, n).astype(jnp.bfloat16).reshape(give.shape[1:])
+                go(swap(n))
+        with jax.named_scope("first#q=%d" % q):
+            for n in mine:
+                first(n)
+        if q == 0:
+            scoped("after_h_2", after_h, 2, 0)
+        if q == 1:
+            scoped("after_h_2", after_h, 2, 1)
+        if q:
+            with jax.named_scope("second#q=%d" % (q - 1)):
+                for n in mine:
+                    second(n - each)
+    with jax.named_scope("last#q=0"):
+        for n in range(2 * each):
+            last(n)
+    with jax.named_scope("second#q=3"):
+        for n in range(3 * each, count):
+            second(n)
+    with jax.named_scope("last#q=1"):
+        for n in range(2 * each, count):
+            last(n)
+
+    with jax.named_scope("drain"):
+        for copy in sent:
+            copy.wait_send()
+        edges(lambda copy: copy.wait_send())
 
 
 def by_group(
@@ -869,7 +1004,7 @@
     feat = pool_weight.shape[1] // 4
     columns = 3 * hw
     half, span, everything = block // 2, 2 * block, 4 * block
-    count = 4
+    count, pieces = 8, 4
     tile = width // count
     f32, bf16 = jnp.float32, jnp.bfloat16
     dma = pltpu.SemaphoreType.DMA
@@ -886,7 +1021,7 @@
         out_specs=vmem,
         scratch_shapes=[
             pltpu.VMEM((everything, width), bf16),
-            pltpu.VMEM((everything, width), bf16),
+            pltpu.VMEM((everything + 16, width), bf16),
             pltpu.VMEM((3, width, columns), bf16),
             pltpu.VMEM((3, 3, rows, columns), bf16),
             pltpu.VMEM((3, rows, columns), bf16),
@@ -898,15 +1033,18 @@
             pltpu.VMEM((everything, hw), bf16),
             pltpu.VMEM((2, span + 16, feat), f32),
             pltpu.VMEM((everything, columns), bf16),
+            pltpu.VMEM((2, 2, hw, span), f32),
+            pltpu.VMEM((2, 8, span), f32),
+            pltpu.VMEM((2, hw, span), bf16),
+            pltpu.VMEM((4, 8, block), f32),
             pltpu.VMEM((128, span), f32),
             pltpu.VMEM((span, 128), f32),
-            pltpu.VMEM((16, span), f32),
-            pltpu.VMEM((8, 128), f32),
-            pltpu.VMEM((8, 128), f32),
-            pltpu.VMEM((2, hw + 8, hw), f32),
-            pltpu.VMEM((2, hw + 8, hw), f32),
-            pltpu.VMEM((2, 8, feat), f32),
-            pltpu.VMEM((2, 8, feat), f32),
+            pltpu.VMEM((2, 8, span), f32),
+            pltpu.VMEM((3, 8, hw), f32),
+            pltpu.VMEM((3, 8, hw), f32),
+            pltpu.VMEM((2, hw, hw), bf16),
+            pltpu.VMEM((2, hw, hw), bf16),
+            pltpu.VMEM((2, 8, width), bf16),
             pltpu.VMEM((count, 4, half, tile), bf16),
             pltpu.VMEM((count, 4, half, tile), bf16),
             pltpu.VMEM((count, 4, half, tile), f32),
@@ -920,12 +1058,13 @@
             dma((3, 2)), dma((3, 2)),
             dma((3, 2, 2)), dma((3, 2, 2)),
             dma((3, 4, 2)), dma((3, 4, 2)),
-            dma((2,)), dma((2,)),
-            dma((2, 2)), dma((2, 2)),
-            dma((3, 2)), dma((3, 2)),
+            dma((pieces,)), dma((pieces,)),
+            dma((2, pieces)), dma((2, pieces)),
+            dma((3, pieces)), dma((3, pieces)),
             dma((3,)), dma((3,)),
             dma((2,)), dma((2,)),
-            dma((3,)), dma((3,)),
+            dma((2,)), dma((2,)),
+            dma((3,)), dma((2,)),
             dma((count,)), dma((count,)),
             dma((count, 2)), dma((count, 2)),
             dma((count,)), dma((count,)),

time: 107 us -> 94.6 us (0.88)
  Pallas kernels: 105 us -> 91.8 us
    pallas_call x1, Pallas kernels: 105 us -> 91.8 us  [by_group(): pl.pallas_call(functools.partial(layer_kernel, n_sp), out_shape=jax.Shape...]
where the time goes in v2:
time: 94.6 us; the launch traced here: 93.7 us
  Pallas kernels  91.8 us (97%)
  local copies, waits for them, and re-layouts  1.88 us (2%)
    pallas_call x1, Pallas kernels, by_group(): pl.pallas_call(functools.partial(layer_kernel, n_sp), out_shape=jax.Shape...  91.8 us

profile of v2, /device:TPU:0, one launch (start us, length us, event | category | flops | bytes accessed | tf_op | source)
XLA Modules:
  0.0 93.7 jit_solution(13659806636711634247)
XLA Ops:
  0.0 91.8 %layer.1 = bf16[128,2048]{1,0:T(8,128)(2,1)} custom-call(bf16[256,2048]{1,0:T(8,128)(2,1)} %bitcast.7, f32[1,2048]{1,0:T(1,128)} %bitcast.9, bf16[128,512]{1,0:T(8,128)(2,1)} %qw.1, bf16[128,512]{1,0:T(8,128)(2,1)} %kw.1, bf16[128,512]{1,0:T(8,128)(2,1)} %vw.1, bf16[128,512]{1,0:T(8,128)(2,1)} %ow.1, bf16[4,4,2048]{2,1,0:T(4,128)(2,1)} %gate_ref.1, ...), custom_call_target="tpu_custom_call" | custom-call | tf_op jit(solution)/shard_map/layer/pallas_call | solution.py:1014
  91.8 1.9 %copy.17 = bf16[1,128,2048]{2,1,0:T(8,128)(2,1)} copy(bf16[1,128,2048]{2,1,0:T(8,128)(2,1)} %bitcast.6) | data formatting | bytes 1048576

commit v3 on v2

--- a/solution.py
+++ b/solution.py
@@ -359,11 +359,11 @@
     n_sp,
     token_ref, gain_ref, qw, kw, vw, ow, gate_ref, bias_ref, decay_ref, mem_ref, nrm_ref,
     hgain_ref, pw, mw, fw,
-    o_ref,
-    x_all, normed, w_all, stage, transit, gmat, dec, init, nrm, proj_a, proj_b, pool_buf, act,
+    out_ref,
+    o_ref, x_all, normed, w_all, stage, transit, gmat, dec, init, nrm, proj_a, ungated, pool_buf, act,
     within, dens, values_t, pre_rows, flat, cols, run_rows, aux_out, aux_in, state_out, state_in, halo_tok,
     give, take, total, s1, l1, s2, l2,
-    loc_w, loc_s, x_ss, x_rs, p_ss, p_rs, h_ss, h_rs, y_ss, y_rs,
+    loc_w, loc_s, out_sem, x_ss, x_rs, p_ss, p_rs, h_ss, h_rs, y_ss, y_rs,
     token_p_ss, token_p_rs, tx_ss, tx_rs, tw_ss, tw_rs, d_ss, d_rs, i_ss, i_rs, m_ss, m_rs, e_ss, e_rs,
     sw_ss, sw_rs, r1_ss, r1_rs, r2_ss, r2_rs,
 ):
@@ -373,7 +373,7 @@
     feat = pw.shape[1] // 4
     half = block // 2
     span = 2 * block
-    pieces_t = token_p_ss.shape[0]
+    pieces_t = token_p_rs.shape[0]
     part = half // pieces_t
     z, fs, c = lax.axis_index("sp"), lax.axis_index("fs"), lax.axis_index("tp")
     y, x = fs // 2, lax.rem(fs, 2)
@@ -396,7 +396,7 @@
     def at(start, size):
         return pl.ds(pl.multiple_of(start, size), size)
 
-    inner = p != h
+    inner, outer = p != h, p == h
     to_m = {"sp": n_sp - 1 - z}
     barrier = pltpu.get_barrier_semaphore()
     for device in (to_x, to_y, to_p, to_h, to_c):
@@ -424,7 +424,7 @@
                     dst = w_all.at[g, row_block(z, y, x), columns]
                 copies.append(
                     pltpu.make_async_copy(
-                        ref.at[:, at(quarters[slot] * size, size)], dst, loc_w.at[g, slot, i]
+                        ref.at[:, at(quarters[slot] * size, size)], dst, loc_w.at[g, slot]
                     )
                 )
                 start += size
@@ -450,34 +450,37 @@
             dst = w_all.at[g, row_block(z, y, 1 - x if incoming else x)]
         else:
             dst = transit.at[g]
-        return remote(dst if incoming else stage.at[g, s], dst, x_ss.at[g, s], x_rs.at[g, s], to_x)
+        return remote(dst if incoming else stage.at[g, s], dst, x_ss, x_rs.at[g, s], to_x)
 
     def p_copy(g, s, incoming=False):
         dst = w_all.at[g, row_block(zn if incoming else z, y, 1 - x if s else x)]
         src = dst if incoming else (transit.at[g] if s else stage.at[g, 2])
-        return remote(src, dst, p_ss.at[g, s], p_rs.at[g, s], to_p)
+        return remote(src, dst, p_ss, p_rs.at[g, s], to_p)
+
+    def h_plane(g, e, s, incoming=False):
+        source = 2 * (1 - h if incoming else h) + e
+        ref = w_all.at[g, row_block(source, y, 1 - x if s else x)]
+        return remote(ref, ref, h_ss, h_rs.at[g, e, s], to_h)
 
     def h_copy(g, k, s, incoming=False):
-        source = (zf, zfn)[k] if incoming else (z, zn)[k]
-        ref = w_all.at[g, row_block(source, y, 1 - x if s else x)]
-        return remote(ref, ref, h_ss.at[g, k, s], h_rs.at[g, k, s], to_h)
+        return h_plane(g, 1 - p if k else p, s, incoming)
 
     def y_copy(g, plane, s, incoming=False):
         ref = w_all.at[g, row_block(plane, 1 - y if incoming else y, 1 - x if s else x)]
-        return remote(ref, ref, y_ss.at[g, plane, s], y_rs.at[g, plane, s], to_y)
-
-    sent = []
+        return remote(ref, ref, y_ss, y_rs.at[2 + plane if g == 2 else g], to_y)
 
     def go(copy):
         copy.start()
-        sent.append(copy)
 
     def ready(g, slots):
-        size = len(groups[g])
-        for place, slot in enumerate((1, 2, 3, 0)):
-            if slot in slots:
-                for copy in locals_[g][place * size : (place + 1) * size]:
-                    copy.wait()
+        for slot in slots:
+            ref = stage.at[g, slot - 1] if slot else w_all.at[g, row_block(z, y, x)]
+            pltpu.make_async_copy(ref, ref, loc_w.at[g, slot]).wait()
+
+    def go_if(here, copy):
+        @pl.when(here)
+        def _():
+            copy.start()
 
     def begin_x(g):
         ready(g, (1, 2))
@@ -488,26 +491,33 @@
         ready(g, (3,))
         go(p_copy(g, 0))
 
-    def begin_h(g):
-        go(h_copy(g, 0, 0))
-
-    def begin_z(g):
-        begin_p(g)
-        if g == 0:
-            ready(g, (0,))
-        begin_h(g)
-
     def begin_y(g):
-        if g:
-            ready(g, (0,))
+        ready(g, (0,))
         go(y_copy(g, z, 0))
 
     def after_x(g):
         x_copy(g, 1, True).wait_recv()
         go(p_copy(g, 1))
         x_copy(g, 0, True).wait_recv()
-        go(h_copy(g, 0, 1))
         go(y_copy(g, z, 1))
+
+    def after_p_y(g):
+        for s in range(2):
+            p_copy(g, s, True).wait_recv()
+            go(y_copy(g, zn, s))
+
+    def all_far_if(here, g):
+        @pl.when(here)
+        def _():
+            for e in range(2):
+                for s in range(2):
+                    h_plane(g, e, s).start()
+
+    def far_if(here, g):
+        @pl.when(here)
+        def _():
+            for s in range(2):
+                h_copy(g, 0, s).start()
 
     def after_p(g):
         for s in range(2):
@@ -520,13 +530,20 @@
             h_copy(g, k, s, True).wait_recv()
             go(y_copy(g, (zf, zfn)[k], s))
 
+    def after_plane(g, e):
+        for s in range(2):
+            h_plane(g, e, s, True).wait_recv()
+            go(y_copy(g, 2 * (1 - h) + e, s))
+
+    def arrived_y(ref, sem):
+        remote(ref, ref, y_ss, sem, to_y).wait_recv()
+
     def after_y(g, plane):
-        for s in range(2):
-            y_copy(g, plane, s, True).wait_recv()
+        start = pl.multiple_of((plane * 4 + 2 * (1 - y)) * rows, rows)
+        arrived_y(w_all.at[g, pl.ds(start, 2 * rows)], y_rs.at[2 + plane])
 
     def all_y(g):
-        for plane in (z, zn, zf, zfn):
-            after_y(g, plane)
+        arrived_y(w_all.at[g, pl.ds(0, 8 * rows)], y_rs.at[g])
 
     def token_rows(j, b, side, i):
         return at((2 * j + b) * block + side * half + i * part, part)
@@ -535,20 +552,20 @@
         b = 1 - p if incoming else p
         dst = x_all.at[token_rows(x, b, c, i)]
         src = dst if incoming else token_ref.at[at(c * half + i * part, part)]
-        return remote(src, dst, token_p_ss.at[i], token_p_rs.at[i], to_p)
+        return remote(src, dst, token_p_ss, token_p_rs.at[i], to_p)
 
     def token_x(kind, i, incoming=False):
         b = 1 - p if kind else p
         dst = x_all.at[token_rows(1 - x if incoming else x, b, c, i)]
         src = dst if incoming or kind else token_ref.at[at(c * half + i * part, part)]
-        return remote(src, dst, tx_ss.at[kind, i], tx_rs.at[kind, i], to_x)
+        return remote(src, dst, tx_ss, tx_rs.at[kind, i], to_x)
 
     places = ((x, 1 - p), (1 - x, p), (1 - x, 1 - p))
 
     def token_swap(which, i, incoming=False):
         j, b = places[which]
         ref = x_all.at[token_rows(j, b, other if incoming else c, i)]
-        return remote(ref, ref, tw_ss.at[which, i], tw_rs.at[which, i], to_c)
+        return remote(ref, ref, tw_ss, tw_rs.at[which], to_c)
 
     edge_rows = halo_tok.shape[1]
 
@@ -623,9 +640,10 @@
             go(token_swap(1 + kind, i))
 
     def swapped(which):
-        for i in range(pieces_t):
-            token_swap(which, i, True).wait_recv()
-        normalise(*places[which])
+        j, b = places[which]
+        ref = x_all.at[at((2 * j + b) * block + other * half, half)]
+        remote(ref, ref, tw_ss, tw_rs.at[which], to_c).wait_recv()
+        normalise(j, b)
 
     def pick_gates():
         gmat[...] = jnp.zeros_like(gmat)
@@ -641,8 +659,9 @@
 
     scoped("barrier", pl.semaphore_wait, barrier, 5 + inner.astype(jnp.int32))
     begin_x(0)
-    begin_z(0)
+    begin_p(0)
     begin_y(0)
+    go(h_copy(0, 0, 0))
     edges(lambda copy: copy.start())
     own_decay.wait()
     go(decay_p())
@@ -656,13 +675,20 @@
     scoped("tok_own", own_tokens.wait)
     scoped("norm_own", normalise, x, p)
     scoped("after_x_0", after_x, 0)
+    go(h_copy(0, 0, 1))
+    early = 2
+    for i in range(1, early):
+        go_if(outer, token_p(i))
     remote(halo_tok.at[x], halo_tok.at[x], e_ss.at[0], e_rs.at[0], to_h).wait_recv()
     go(edge_x())
     scoped("after_p_0", after_p, 0)
-    for i in range(1, pieces_t):
+    for i in range(1, early):
+        go_if(inner, token_p(i))
+    for i in range(early, pieces_t):
         go(token_p(i))
-    begin_z(1)
+    begin_p(1)
     scoped("after_x_1", after_x, 1)
+    far_if(outer, 1)
     scoped("after_h_0", after_h, 0, 0)
     scoped("tok_p", token_arrivals_p, (0,))
     scoped("tok_x0", token_arrivals_x, 0, (0, 1))
@@ -670,6 +696,7 @@
     scoped("tok_p", token_arrivals_p, (1,))
     scoped("tok_x0", token_arrivals_x, 0, (2, 3))
     scoped("norm_x", swapped, 1)
+    far_if(inner, 1)
     edge_x(True).wait_recv()
     normalise_edges()
     scoped("tok_p", token_arrivals_p, (2, 3))
@@ -679,7 +706,13 @@
     go(init_x(1))
     begin_x(2)
     begin_y(2)
+
     scoped("norm_p", swapped, 0)
+
+    @pl.when(outer)
+    def _():
+        scoped("after_p_1", after_p, 1)
+
     scoped("after_y_0", all_y, 0)
 
     def project(g, place, store):
@@ -694,12 +727,20 @@
     for place in ((x, p), places[0], places[1]):
         scoped("project_0", project, 0, place, store_a)
     scoped("tok_x1", token_arrivals_x, 1, (0, 1))
-    scoped("after_p_1", after_p, 1)
+
+    @pl.when(inner)
+    def _():
+        scoped("after_p_1i", after_p, 1)
+
+    begin_p(2)
+
     scoped("tok_x1", token_arrivals_x, 1, (2, 3))
     scoped("after_h_1", after_h, 1, 0)
     scoped("norm_px", swapped, 2)
     decay_x(0, True).wait_recv()
     decay_x(1, True).wait_recv()
+
+    scoped("after_x_2", after_x, 2)
 
     with jax.named_scope("gates"):
         tall = []
@@ -763,8 +804,6 @@
             aux_out[j] = kept * nrm[j, h, pl.ds(quarter, 1), :] + grown[hw:]
     go(message(0))
     go(message(1))
-    begin_p(2)
-    begin_h(2)
 
     with jax.named_scope("levels"):
         flat[16:, :] = jnp.zeros_like(flat[16:, :])
@@ -797,31 +836,12 @@
 
     scoped("attend_0", attend, 0)
     scoped("attend_1", attend, 1)
-    scoped("after_x_2", after_x, 2)
     scoped("after_h_1", after_h, 1, 1)
-    scoped("after_p_2", after_p, 2)
-    scoped("after_y_1", all_y, 1)
-
-    def project_b():
-        for i in range(4):
-            last_rows = 2 * edge_rows if i == 3 else 0
-            value = jnp.dot(
-                normed[i * block : (i + 1) * block + last_rows, :], w_all[1],
-                preferred_element_type=jnp.float32,
-            ).astype(jnp.bfloat16)
-            proj_b[i * block : (i + 1) * block, :] = value[:block, :hw]
-            start = 8 + (i % 2) * block
-            pool_buf[i // 2, start : start + block, :] = value[:block, hw:].astype(jnp.float32)
-        beyond = value[block:, hw:].astype(jnp.float32)
-        zero = jnp.zeros((8, feat), jnp.float32)
-        for j in range(2):
-            mine = beyond[j * edge_rows : (j + 1) * edge_rows]
-            pool_buf[j, 0:8, :] = jnp.where(low, zero, mine[edge_rows - 8 :])
-            pool_buf[j, span + 8 : span + 16, :] = jnp.where(low, mine[:8], zero)
-
-    scoped("project_1", project_b)
+    scoped("after_p_2y", after_p_y, 2)
+    all_far_if(inner, 2)
     scoped("state_in", message(1, True).wait_recv)
     scoped("aux_in", message(0, True).wait_recv)
+    all_far_if(outer, 2)
 
     with jax.named_scope("enter"):
         arrived = aux_in[2, :, 0:1]
@@ -865,18 +885,36 @@
             )
         summed = both[0] + both[1]
         summed = summed * lax.rsqrt(jnp.mean(summed * summed, axis=0, keepdims=True) + norm_eps)
-        out = (
-            summed.T
-            * hgain_ref[pl.ds(quarter, 1), :]
-            * jax.nn.sigmoid(proj_b[j * span : (j + 1) * span, :].astype(jnp.float32))
-        ).astype(jnp.bfloat16)
-        for i in range(4):
-            place = (i % 2) * span + (2 * j + i // 2) * half
-            act[place : place + half, 0:hw] = out[i * half : (i + 1) * half]
+        ungated[j * span : (j + 1) * span, :] = summed.T * hgain_ref[pl.ds(quarter, 1), :]
 
     scoped("finish", finish, 0)
     scoped("finish", finish, 1)
 
+    scoped("after_y_1", all_y, 1)
+
+    def project_b():
+        for i in range(4):
+            last_rows = 2 * edge_rows if i == 3 else 0
+            value = jnp.dot(
+                normed[i * block : (i + 1) * block + last_rows, :], w_all[1],
+                preferred_element_type=jnp.float32,
+            ).astype(jnp.bfloat16)
+            gate = jax.nn.sigmoid(value[:block, :hw].astype(jnp.float32))
+            out = (ungated[i * block : (i + 1) * block, :] * gate).astype(jnp.bfloat16)
+            for e in range(2):
+                act[e * span + i * half : e * span + (i + 1) * half, 0:hw] = out[
+                    e * half : (e + 1) * half
+                ]
+            start = 8 + (i % 2) * block
+            pool_buf[i // 2, start : start + block, :] = value[:block, hw:].astype(jnp.float32)
+        beyond = value[block:, hw:].astype(jnp.float32)
+        zero = jnp.zeros((8, feat), jnp.float32)
+        for j in range(2):
+            mine = beyond[j * edge_rows : (j + 1) * edge_rows]
+            pool_buf[j, 0:8, :] = jnp.where(low, zero, mine[edge_rows - 8 :])
+            pool_buf[j, span + 8 : span + 16, :] = jnp.where(low, mine[:8], zero)
+
+    scoped("project_1", project_b)
     with jax.named_scope("pooling"):
         group = (c * 4 + quarter) * feat * 4 // width
         for k in range(4):
@@ -909,21 +947,21 @@
         return at(planes[n // each] * (width // 4) + (n % each) * tile, tile)
 
     def mixed(n):
-        return n % 2 == 1
+        return n in (3, 5, 7)
 
     def swap(n):
-        return remote(give.at[n], take.at[n], sw_ss.at[n], sw_rs.at[n], to_c)
+        return remote(give.at[n], take.at[n], sw_ss, sw_rs.at[n], to_c)
 
     def first_stage(n, slot, incoming=False):
         dst = l1.at[n, slot]
         return remote(
-            dst if incoming else s1.at[n, slot], dst, r1_ss.at[n, slot], r1_rs.at[n, slot],
+            dst if incoming else s1.at[n, slot], dst, r1_ss, r1_rs.at[n, slot],
             to_p if mixed(n) else to_x,
         )
 
     def second_stage(n, incoming=False):
         return remote(
-            l2.at[n] if incoming else s2.at[n], l2.at[n], r2_ss.at[n], r2_rs.at[n],
+            l2.at[n] if incoming else s2.at[n], l2.at[n], r2_ss, r2_rs.at[n],
             to_x if mixed(n) else to_p,
         )
 
@@ -951,15 +989,25 @@
         s2[n] = (total[n, middle] + l1[n, 1].astype(jnp.float32)).astype(jnp.bfloat16)
         go(second_stage(n))
 
+    def out_copy(n):
+        return pltpu.make_async_copy(
+            o_ref.at[:, columns_of(n)], out_ref.at[:, columns_of(n)], out_sem
+        )
+
     def last(n):
         first_stage(n, 0, True).wait_recv()
         second_stage(n, True).wait_recv()
         o_ref[:, columns_of(n)] = (
             total[n, home] + l1[n, 0].astype(jnp.float32) + l2[n].astype(jnp.float32)
         ).astype(jnp.bfloat16)
+        out_copy(n).start()
 
     for q in range(4):
         mine = range(q * each, (q + 1) * each)
+        if q == 2:
+            with jax.named_scope("second#q=1"):
+                for n in range(each, 2 * each):
+                    second(n)
         scoped("plane#q=%d" % q, after_y, 2, planes[q])
         with jax.named_scope("give#q=%d" % q):
             for n in mine:
@@ -968,11 +1016,13 @@
         with jax.named_scope("first#q=%d" % q):
             for n in mine:
                 first(n)
-        if q == 0:
-            scoped("after_h_2", after_h, 2, 0)
         if q == 1:
-            scoped("after_h_2", after_h, 2, 1)
-        if q:
+            scoped("after_h_2", after_plane, 2, 0)
+            with jax.named_scope("second#q=0"):
+                for n in range(each):
+                    second(n)
+            scoped("after_h_2", after_plane, 2, 1)
+        if q > 2:
             with jax.named_scope("second#q=%d" % (q - 1)):
                 for n in mine:
                     second(n - each)
@@ -987,9 +1037,26 @@
             last(n)
 
     with jax.named_scope("drain"):
-        for copy in sent:
+        sends = (
+            (w_all.at[:, 0 : 2 * rows], x_ss),
+            (w_all.at[:, 0 : 2 * rows], p_ss),
+            (w_all.at[:, 0 : 4 * rows], h_ss),
+            (w_all.at[:, 0 : 8 * rows], y_ss),
+            (x_all.at[0:half], token_p_ss),
+            (x_all.at[0 : 2 * half], tx_ss),
+            (x_all.at[0 : 3 * half], tw_ss),
+            (give, sw_ss),
+            (s1, r1_ss),
+            (s2, r2_ss),
+        )
+        for ref, sem in sends:
+            remote(ref, ref, sem, e_rs.at[0], to_x).wait_send()
+        for copy in (
+            decay_p(), decay_x(0), decay_x(1), init_x(0), init_x(1), message(0), message(1), edge_x()
+        ):
             copy.wait_send()
         edges(lambda copy: copy.wait_send())
+        pltpu.make_async_copy(o_ref, out_ref, out_sem).wait()
 
 
 def by_group(
@@ -1018,8 +1085,9 @@
             anywhere, vmem, anywhere, anywhere, anywhere, anywhere, vmem, smem, anywhere, anywhere,
             anywhere, vmem, anywhere, anywhere, anywhere,
         ],
-        out_specs=vmem,
+        out_specs=anywhere,
         scratch_shapes=[
+            pltpu.VMEM((half, width), bf16),
             pltpu.VMEM((everything, width), bf16),
             pltpu.VMEM((everything + 16, width), bf16),
             pltpu.VMEM((3, width, columns), bf16),
@@ -1030,7 +1098,7 @@
             pltpu.VMEM((2, hw, hw), f32),
             pltpu.VMEM((2,) + init_normalizer.shape[1:], f32),
             pltpu.VMEM((everything, columns), bf16),
-            pltpu.VMEM((everything, hw), bf16),
+            pltpu.VMEM((everything, hw), f32),
             pltpu.VMEM((2, span + 16, feat), f32),
             pltpu.VMEM((everything, columns), bf16),
             pltpu.VMEM((2, 2, hw, span), f32),
@@ -1052,22 +1120,23 @@
             pltpu.VMEM((count, 2, half, tile), bf16),
             pltpu.VMEM((count, half, tile), bf16),
             pltpu.VMEM((count, half, tile), bf16),
-            dma((3, 4, 3)),
+            dma((3, 4)),
             dma((4,)),
-            dma((3, 2)), dma((3, 2)),
-            dma((3, 2)), dma((3, 2)),
-            dma((3, 2, 2)), dma((3, 2, 2)),
-            dma((3, 4, 2)), dma((3, 4, 2)),
-            dma((pieces,)), dma((pieces,)),
-            dma((2, pieces)), dma((2, pieces)),
-            dma((3, pieces)), dma((3, pieces)),
+            dma(()),
+            dma(()), dma((3, 2)),
+            dma(()), dma((3, 2)),
+            dma(()), dma((3, 2, 2)),
+            dma(()), dma((6,)),
+            dma(()), dma((pieces,)),
+            dma(()), dma((2, pieces)),
+            dma(()), dma((3,)),
             dma((3,)), dma((3,)),
             dma((2,)), dma((2,)),
             dma((2,)), dma((2,)),
             dma((3,)), dma((2,)),
-            dma((count,)), dma((count,)),
-            dma((count, 2)), dma((count, 2)),
-            dma((count,)), dma((count,)),
+            dma(()), dma((count,)),
+            dma(()), dma((count, 2)),
+            dma(()), dma((count,)),
         ],
         compiler_params=pltpu.CompilerParams(
             collective_id=0, has_side_effects=True, vmem_limit_bytes=60 * 2**20

time: 94.6 us -> 89.3 us (0.944)
  Pallas kernels: 91.8 us -> 87.2 us
    pallas_call x1, Pallas kernels: 91.8 us -> 87.2 us  [by_group(): pl.pallas_call(functools.partial(layer_kernel, n_sp), out_shape=jax.Shape...]
where the time goes in v3:
time: 89.3 us; the launch traced here: 89.1 us
  Pallas kernels  87.2 us (98%)
  local copies, waits for them, and re-layouts  1.88 us (2%)
    pallas_call x1, Pallas kernels, by_group(): pl.pallas_call(functools.partial(layer_kernel, n_sp), out_shape=jax.Shape...  87.2 us
    unnamed x1, local copies, waits for them, and re-layouts  1.88 us

profile of v3, /device:TPU:0, one launch (start us, length us, event | category | flops | bytes accessed | tf_op | source)
XLA Modules:
  0.0 89.1 jit_solution(118607599029443063)
XLA Ops:
  0.0 87.2 %layer.1 = bf16[128,2048]{1,0:T(8,128)(2,1)} custom-call(bf16[256,2048]{1,0:T(8,128)(2,1)} %bitcast.7, f32[1,2048]{1,0:T(1,128)} %bitcast.9, bf16[128,512]{1,0:T(8,128)(2,1)} %qw.1, bf16[128,512]{1,0:T(8,128)(2,1)} %kw.1, bf16[128,512]{1,0:T(8,128)(2,1)} %vw.1, bf16[128,512]{1,0:T(8,128)(2,1)} %ow.1, bf16[4,4,2048]{2,1,0:T(4,128)(2,1)} %gate_ref.1, ...), custom_call_target="tpu_custom_call" | custom-call | tf_op jit(solution)/shard_map/layer/pallas_call | solution.py:1081
  87.2 1.9 %copy.17 = bf16[1,128,2048]{2,1,0:T(8,128)(2,1)} copy(bf16[1,128,2048]{2,1,0:T(8,128)(2,1)} %bitcast.6) | data formatting | bytes 1048576

commit v4 on v3

--- a/solution.py
+++ b/solution.py
@@ -357,19 +357,19 @@
 
 def layer_kernel(
     n_sp,
-    token_ref, gain_ref, qw, kw, vw, ow, gate_ref, bias_ref, decay_ref, mem_ref, nrm_ref,
-    hgain_ref, pw, mw, fw,
-    out_ref,
-    o_ref, x_all, normed, w_all, stage, transit, gmat, dec, init, nrm, proj_a, ungated, pool_buf, act,
+    token_ref, gain_hbm, qw, kw, vw, ow, gate_hbm, bias_hbm, decay_ref, mem_ref, nrm_ref,
+    hgain_hbm, pw, mw, fw,
+    o_ref,
+    gain_ref, gate_ref, bias_ref, hgain_ref, x_all, normed, w_all, stage, transit, gmat, dec, init, nrm, proj_a, ungated, pool_buf, act,
     within, dens, values_t, pre_rows, flat, cols, run_rows, aux_out, aux_in, state_out, state_in, halo_tok,
     give, take, total, s1, l1, s2, l2,
-    loc_w, loc_s, out_sem, x_ss, x_rs, p_ss, p_rs, h_ss, h_rs, y_ss, y_rs,
+    loc_w, loc_s, small_sem, x_ss, x_rs, p_ss, p_rs, h_ss, h_rs, y_ss, y_rs,
     token_p_ss, token_p_rs, tx_ss, tx_rs, tw_ss, tw_rs, d_ss, d_rs, i_ss, i_rs, m_ss, m_rs, e_ss, e_rs,
     sw_ss, sw_rs, r1_ss, r1_rs, r2_ss, r2_rs,
 ):
     block, width = token_ref.shape
     rows = qw.shape[0]
-    hw = hgain_ref.shape[1]
+    hw = hgain_hbm.shape[1]
     feat = pw.shape[1] // 4
     half = block // 2
     span = 2 * block
@@ -430,6 +430,15 @@
                 start += size
         return copies
 
+    small = [
+        pltpu.make_async_copy(src, dst, small_sem.at[i])
+        for i, (src, dst) in enumerate(
+            (
+                (gain_hbm, gain_ref), (gate_hbm, gate_ref), (bias_hbm, bias_ref),
+                (hgain_hbm, hgain_ref),
+            )
+        )
+    ]
     locals_ = [local_weights(g) for g in range(3)]
     own_tokens = pltpu.make_async_copy(
         token_ref, x_all.at[at((2 * x + p) * block, block)], loc_s.at[0]
@@ -442,7 +451,7 @@
     own_tokens.start()
     for copy in locals_[1] + locals_[2]:
         copy.start()
-    for copy in (own_decay, own_init, own_nrm):
+    for copy in small + [own_decay, own_init, own_nrm]:
         copy.start()
 
     def x_copy(g, s, incoming=False):
@@ -671,6 +680,8 @@
     for i in range(pieces_t):
         go(token_x(0, i))
     begin_y(1)
+    for copy in small:
+        copy.wait()
     scoped("pick", pick_gates)
     scoped("tok_own", own_tokens.wait)
     scoped("norm_own", normalise, x, p)
@@ -735,7 +746,11 @@
     begin_p(2)
 
     scoped("tok_x1", token_arrivals_x, 1, (2, 3))
-    scoped("after_h_1", after_h, 1, 0)
+
+    @pl.when(inner)
+    def _():
+        scoped("after_h_1i", after_h, 1, 0)
+
     scoped("norm_px", swapped, 2)
     decay_x(0, True).wait_recv()
     decay_x(1, True).wait_recv()
@@ -775,6 +790,10 @@
         dst = (aux_in, state_in)[which]
         return remote(dst if incoming else src, dst, m_ss.at[which], m_rs.at[which], to_h)
 
+    @pl.when(outer)
+    def _():
+        scoped("after_h_1", after_h, 1, 0)
+
     scoped("project_0", project, 0, places[2], store_a)
 
     with jax.named_scope("state"):
@@ -989,18 +1008,12 @@
         s2[n] = (total[n, middle] + l1[n, 1].astype(jnp.float32)).astype(jnp.bfloat16)
         go(second_stage(n))
 
-    def out_copy(n):
-        return pltpu.make_async_copy(
-            o_ref.at[:, columns_of(n)], out_ref.at[:, columns_of(n)], out_sem
-        )
-
     def last(n):
         first_stage(n, 0, True).wait_recv()
         second_stage(n, True).wait_recv()
         o_ref[:, columns_of(n)] = (
             total[n, home] + l1[n, 0].astype(jnp.float32) + l2[n].astype(jnp.float32)
         ).astype(jnp.bfloat16)
-        out_copy(n).start()
 
     for q in range(4):
         mine = range(q * each, (q + 1) * each)
@@ -1026,12 +1039,12 @@
             with jax.named_scope("second#q=%d" % (q - 1)):
                 for n in mine:
                     second(n - each)
+    with jax.named_scope("second#q=3"):
+        for n in range(3 * each, count):
+            second(n)
     with jax.named_scope("last#q=0"):
         for n in range(2 * each):
             last(n)
-    with jax.named_scope("second#q=3"):
-        for n in range(3 * each, count):
-            second(n)
     with jax.named_scope("last#q=1"):
         for n in range(2 * each, count):
             last(n)
@@ -1056,7 +1069,6 @@
         ):
             copy.wait_send()
         edges(lambda copy: copy.wait_send())
-        pltpu.make_async_copy(o_ref, out_ref, out_sem).wait()
 
 
 def by_group(
@@ -1075,19 +1087,17 @@
     tile = width // count
     f32, bf16 = jnp.float32, jnp.bfloat16
     dma = pltpu.SemaphoreType.DMA
-    vmem = pl.BlockSpec(memory_space=pltpu.VMEM)
     anywhere = pl.BlockSpec(memory_space=pl.ANY)
-    smem = pl.BlockSpec(memory_space=pltpu.SMEM)
     mixed = pl.pallas_call(
         functools.partial(layer_kernel, n_sp),
-        out_shape=jax.ShapeDtypeStruct((half, width), bf16),
-        in_specs=[
-            anywhere, vmem, anywhere, anywhere, anywhere, anywhere, vmem, smem, anywhere, anywhere,
-            anywhere, vmem, anywhere, anywhere, anywhere,
-        ],
-        out_specs=anywhere,
+        out_shape=pltpu.VMEM((half, width), bf16),
+        in_specs=[anywhere] * 15,
+        out_specs=pl.BlockSpec(memory_space=pltpu.VMEM),
         scratch_shapes=[
-            pltpu.VMEM((half, width), bf16),
+            pltpu.VMEM((1, width), f32),
+            pltpu.VMEM(gate_weight.shape, bf16),
+            pltpu.SMEM(gate_bias.shape, f32),
+            pltpu.VMEM(head_gain.shape, f32),
             pltpu.VMEM((everything, width), bf16),
             pltpu.VMEM((everything + 16, width), bf16),
             pltpu.VMEM((3, width, columns), bf16),
@@ -1122,7 +1132,7 @@
             pltpu.VMEM((count, half, tile), bf16),
             dma((3, 4)),
             dma((4,)),
-            dma(()),
+            dma((4,)),
             dma(()), dma((3, 2)),
             dma(()), dma((3, 2)),
             dma(()), dma((3, 2, 2)),

time: 89.3 us -> 87 us (0.974)
  Pallas kernels: 87.2 us -> 86.1 us
  local copies, waits for them, and re-layouts: 1.88 us -> 0.8 us
    pallas_call x1, Pallas kernels: 87.2 us -> 86.1 us  [by_group(): pl.pallas_call(functools.partial(layer_kernel, n_sp), out_shape=pltpu.VME...]
    unnamed x1, local copies, waits for them, and re-layouts: 1.88 us -> 0.8 us
where the time goes in v4:
time: 87 us; the launch traced here: 86.9 us
  Pallas kernels  86.1 us (99%)
    pallas_call x1, Pallas kernels, by_group(): pl.pallas_call(functools.partial(layer_kernel, n_sp), out_shape=pltpu.VME...  86.1 us

profile of v4, /device:TPU:0, one launch (start us, length us, event | category | flops | bytes accessed | tf_op | source)
XLA Modules:
  0.0 86.9 jit_solution(13603644829039401880)
XLA Ops:
  0.0 86.1 %layer.1 = bf16[128,2048]{1,0:T(8,128)(2,1)S(1)} custom-call(bf16[256,2048]{1,0:T(8,128)(2,1)} %bitcast.7, f32[1,2048]{1,0:T(1,128)} %bitcast.9, bf16[128,512]{1,0:T(8,128)(2,1)} %qw.1, bf16[128,512]{1,0:T(8,128)(2,1)} %kw.1, bf16[128,512]{1,0:T(8,128)(2,1)} %vw.1, bf16[128,512]{1,0:T(8,128)(2,1)} %ow.1, bf16[4,4,2048]{2,1,0:T(4,128)(2,1)} %gate_hbm.1, ...), custom_call_target="tpu_custom_call" | custom-call | tf_op jit(solution)/shard_map/layer/pallas_call | solution.py:1091
  86.1 0.8 copy.17

commit v5 on v4

--- a/solution.py
+++ b/solution.py
@@ -508,7 +508,10 @@
         x_copy(g, 1, True).wait_recv()
         go(p_copy(g, 1))
         x_copy(g, 0, True).wait_recv()
-        go(y_copy(g, z, 1))
+        if g < 2:
+            go(y_copy(g, z, 1))
+        else:
+            go_if(inner, y_copy(g, z, 1))
 
     def after_p_y(g):
         for s in range(2):
@@ -856,7 +859,9 @@
     scoped("attend_0", attend, 0)
     scoped("attend_1", attend, 1)
     scoped("after_h_1", after_h, 1, 1)
+    go_if(outer & (p == 0), y_copy(2, z, 1))
     scoped("after_p_2y", after_p_y, 2)
+    go_if(outer & (p == 1), y_copy(2, z, 1))
     all_far_if(inner, 2)
     scoped("state_in", message(1, True).wait_recv)
     scoped("aux_in", message(0, True).wait_recv)

time: 87 us -> 87 us (level)
  no operation moved by 1% of the time
where the time goes in v5:
time: 87 us; the launch traced here: 86.9 us
  Pallas kernels  86.1 us (99%)
    pallas_call x1, Pallas kernels, by_group(): pl.pallas_call(functools.partial(layer_kernel, n_sp), out_shape=pltpu.VME...  86.1 us

profile of v5, /device:TPU:0, one launch (start us, length us, event | category | flops | bytes accessed | tf_op | source)
XLA Modules:
  0.0 86.9 jit_solution(13405234415351243245)
XLA Ops:
  0.0 86.1 %layer.1 = bf16[128,2048]{1,0:T(8,128)(2,1)S(1)} custom-call(bf16[256,2048]{1,0:T(8,128)(2,1)} %bitcast.7, f32[1,2048]{1,0:T(1,128)} %bitcast.9, bf16[128,512]{1,0:T(8,128)(2,1)} %qw.1, bf16[128,512]{1,0:T(8,128)(2,1)} %kw.1, bf16[128,512]{1,0:T(8,128)(2,1)} %vw.1, bf16[128,512]{1,0:T(8,128)(2,1)} %ow.1, bf16[4,4,2048]{2,1,0:T(4,128)(2,1)} %gate_hbm.1, ...), custom_call_target="tpu_custom_call" | custom-call | tf_op jit(solution)/shard_map/layer/pallas_call | solution.py:1096
  86.1 0.8 copy.17
